TPU v7x, 32 devices: a whole 2x2x4 slice. The times are simulated.
32 devices in a mesh: kv: 8 (over z, y), tp: 4 (over x, core).
Axes of the slice: x: 2, y: 2, z: 4, core: 2. Of those that a mesh axis runs over, the one named last changes fastest.
Arguments:
- tokens: bfloat16 [64, 4096], P(None, 'kv'), may hold values from -8 to 8
- attn_gain: float32 [4096], P('kv'), may hold values from 0.1 to 1.9
- w_query: bfloat16 [4096, 2048], P('kv', 'tp'), may hold values from -0.09375 to 0.09375
- w_key: bfloat16 [4096, 2048], P('kv', 'tp'), may hold values from -0.09375 to 0.09375
- w_value: bfloat16 [4096, 4096], P('kv', 'tp'), may hold values from -0.09375 to 0.09375
- w_outgate: bfloat16 [4096, 4096], P('kv', 'tp'), may hold values from -0.09375 to 0.09375
- w_gates: bfloat16 [4096, 16], replicated, may hold values from -0.029907227 to 0.029907227
- forget_bias: float32 [8], replicated, may hold values from -1 to 3
- state_c: float32 [64, 8, 512, 256], P('kv', 'tp'), may hold values from -6 to 6
- state_n: float32 [64, 8, 256], P('kv', 'tp'), may hold values from -6 to 6
- state_m: float32 [64, 8], P('kv', 'tp'), may hold values from -2 to 0.5
- w_output: bfloat16 [4096, 4096], P('tp', 'kv'), may hold values from -0.09375 to 0.09375
- mlp_gain: float32 [4096], P('kv'), may hold values from 0.1 to 1.9
- w_gateff: bfloat16 [4096, 11008], P('kv', 'tp'), may hold values from -0.09375 to 0.09375
- w_upff: bfloat16 [4096, 11008], P('kv', 'tp'), may hold values from -0.09375 to 0.09375
- w_downff: bfloat16 [11008, 4096], P('tp', 'kv'), may hold values from -0.0546875 to 0.0546875
Outputs:
- mixed: bfloat16 [64, 4096], P(None, 'kv')
- new_c: float32 [64, 8, 512, 256], P('kv', 'tp')
- new_n: float32 [64, 8, 256], P('kv', 'tp')
- new_m: float32 [64, 8], P('kv', 'tp')
All inputs are finite; a program needn't handle non-finite values.
Results may differ from a plain program's by a relative error of at most 0.0083.
Values may be sent and summed in bfloat16 or wider, within the bound.
A program may use at most 64 MiB of HBM per device.

v0:
```python
import jax
import jax.numpy as jnp
from jax import lax
from jax.experimental import pallas as pl
from jax.experimental.pallas import tpu as pltpu
from jax.sharding import PartitionSpec as P

norm_floor = 1e-05
MESH = pl.DeviceIdType.MESH
LANES = 128
CHUNK = 512
SPANS = 4
VMEM_ALL = 67043328
SLACK = 640 * 1024
VMEM_SPEC = pl.BlockSpec(memory_space=pltpu.VMEM)
HBM_SPEC = pl.BlockSpec(memory_space=pltpu.HBM)


def pieces(total):
    return [(at, min(CHUNK, total - at)) for at in range(0, total, CHUNK)]


def peer_of(axis, step):
    count = lax.axis_size(axis)
    return lax.rem(lax.axis_index(axis) + step, count)


def signal_peers(barrier, axis):
    for step in range(1, lax.axis_size(axis)):
        pl.semaphore_signal(
            barrier, inc=1, device_id={axis: peer_of(axis, step)}, device_id_type=MESH
        )


def remote(axis, step, src, dst, send_sem, recv_sem):
    return pltpu.make_async_remote_copy(
        src_ref=src,
        dst_ref=dst,
        send_sem=send_sem,
        recv_sem=recv_sem,
        device_id={axis: peer_of(axis, step)},
        device_id_type=MESH,
    )


def inner_size(count):
    size = 1 << ((count.bit_length() - 1) // 2)
    return size if count % size == 0 else 1


def place():
    count = lax.axis_size("kv")
    inner = inner_size(count)
    kv = lax.axis_index("kv")
    return kv // inner, kv % inner, count // inner, inner


def inner_peer(step):
    outer_at, inner_at, _, inner = place()
    return (inner_at + step) % inner, outer_at * inner + (inner_at + step) % inner


def outer_peer(step):
    outer_at, inner_at, outer, inner = place()
    return (outer_at + step) % outer, ((outer_at + step) % outer) * inner + inner_at


def send_to(device, src, dst, send_sem, recv_sem):
    copy = pltpu.make_async_remote_copy(
        src_ref=src,
        dst_ref=dst,
        send_sem=send_sem,
        recv_sem=recv_sem,
        device_id={"kv": device},
        device_id_type=MESH,
    )
    copy.start()
    return copy


def scatter_first(i, part, land, columns, send_sem, recv_sem):
    _, _, _, inner = place()
    copies = []
    for step in range(1, inner):
        at, device = inner_peer(step)
        copies.append(
            send_to(
                device, part.at[at, :, :, columns], land.at[step, :, :, columns],
                send_sem.at[i, step], recv_sem.at[i, step],
            )
        )
    return copies


def scatter_second(i, first, part, land, both, last, at, size, send_sem, recv_sem):
    _, inner_at, outer, inner = place()
    columns = pl.ds(at, size)
    for copy in first:
        copy.wait_recv()
    acc = part[inner_at, :, :, at : at + size].astype(jnp.float32)
    for step in range(1, inner):
        acc += land[step, :, :, at : at + size].astype(jnp.float32)
    both[:, :, at : at + size] = acc.astype(jnp.bfloat16)
    copies = []
    for step in range(1, outer):
        to, device = outer_peer(step)
        copies.append(
            send_to(
                device, both.at[to, :, columns], last.at[step, :, columns],
                send_sem.at[i, step], recv_sem.at[i, step],
            )
        )
    return copies


def scatter_sum(second, both, last, at, size):
    outer_at, _, outer, _ = place()
    for copy in second:
        copy.wait_recv()
    acc = both[outer_at, :, at : at + size].astype(jnp.float32)
    for step in range(1, outer):
        acc += last[step, :, at : at + size].astype(jnp.float32)
    return acc


def put_part(part, out, at, size):
    inner, outer, rows, _ = part.shape
    split = out.reshape(outer, inner, rows, size).astype(jnp.bfloat16)
    for i in range(inner):
        part[i, :, :, at : at + size] = split[:, i]


def project_kernel(
    tok_ref, gain_ref, wq, wk, wv, wo, wg,
    proj_ref, gate_ref,
    wq_v, wk_v, wv_v, wo_v, wg_v, part, land, both, last, gpart, gland,
    load_sem, send_sem, recv_sem, send2_sem, recv2_sem, gsend_sem, grecv_sem,
):
    kv = lax.axis_index("kv")
    count = lax.axis_size("kv")
    batch, width = tok_ref.shape
    rows = batch // count
    weights = [(wq, wq_v), (wk, wk_v), (wv, wv_v), (wo, wo_v)]
    loads = [
        pltpu.make_async_copy(wg.at[:, pl.ds(pl.multiple_of(kv * width, LANES), width)], wg_v, load_sem.at[len(weights)])
    ]
    loads += [
        pltpu.make_async_copy(src, dst, load_sem.at[i]) for i, (src, dst) in enumerate(weights)
    ]
    barrier = pltpu.get_barrier_semaphore()
    signal_peers(barrier, "kv")
    for load in loads:
        load.start()
    tok = tok_ref[...].astype(jnp.float32)
    squares = jnp.sum(tok * tok, axis=1, keepdims=True)
    normed = (tok * gain_ref[...]).astype(jnp.bfloat16)
    loads[0].wait()
    gates = lax.dot_general(
        normed, wg_v[...], (((1,), (1,)), ((), ())), preferred_element_type=jnp.float32
    )
    gate_cols = gates.shape[1]
    gpart[...] = jnp.broadcast_to(squares, (batch, LANES)).reshape(count, rows, LANES)
    gpart[:, :, :gate_cols] = gates.reshape(count, rows, gate_cols)
    pl.semaphore_wait(barrier, count - 1)
    copies = []
    for step in range(1, count):
        copy = remote(
            "kv", step, gpart.at[peer_of("kv", step)], gland.at[step],
            gsend_sem.at[step], grecv_sem.at[step],
        )
        copy.start()
        copies.append(copy)
    at = 0
    groups = []
    for i, (_, dst) in enumerate(weights):
        loads[i + 1].wait()
        wide = dst.shape[1]
        for off, size in pieces(wide):
            out = jnp.dot(normed, dst[:, off : off + size], preferred_element_type=jnp.float32)
            put_part(part, out, at + off, size)
        copies_one = scatter_first(i, part, land, pl.ds(at, wide), send_sem, recv_sem)
        groups.append((at, wide, copies_one))
        at += wide
    seconds = [
        scatter_second(i, first, part, land, both, last, at, wide, send2_sem, recv2_sem)
        for i, (at, wide, first) in enumerate(groups)
    ]
    total = gpart[kv]
    for copy in copies:
        copy.wait_recv()
    for step in range(1, count):
        total += gland[step]
    mean = total[:, gate_cols : gate_cols + 1] / (width * count)
    scale = lax.rsqrt(mean + norm_floor)
    gate_ref[...] = total * scale
    for (at, wide, _), second in zip(groups, seconds):
        proj_ref[:, at : at + wide] = scatter_sum(second, both, last, at, wide) * scale
    for copy in copies:
        copy.wait_send()
    for (_, _, first), second in zip(groups, seconds):
        for copy in first + second:
            copy.wait_send()


def state_kernel(
    proj_ref, gate_ref, bias_ref, m_ref, n_ref, c_hbm,
    head_ref, newn_ref, newm_ref, newc_hbm,
    held, in_sem, out_sem,
):
    rows, heads, value_size, query_size = held.shape
    tp = lax.axis_index("tp")
    heads_all = bias_ref.shape[1]
    loads = [
        pltpu.make_async_copy(c_hbm.at[b, h], held.at[b, h], in_sem.at[b, h])
        for h in range(heads)
        for b in range(rows)
    ]
    for load in loads:
        load.start()
    gates = gate_ref[...]
    lane = lax.broadcasted_iota(jnp.int32, gates.shape, 1)
    bias_lane = lax.broadcasted_iota(jnp.int32, bias_ref.shape, 1)
    sub = lax.broadcasted_iota(jnp.int32, (rows, value_size), 0)
    eye = lax.broadcasted_iota(jnp.int32, (rows, rows), 0) == lax.broadcasted_iota(
        jnp.int32, (rows, rows), 1
    )
    query_width = heads * query_size
    value_at = 2 * query_width
    out_at = value_at + heads * value_size
    stores = []
    for h in range(heads):
        column = tp * heads + h
        log_input = jnp.sum(jnp.where(lane == column, gates, 0.0), axis=1, keepdims=True)
        forget = jnp.sum(jnp.where(lane == heads_all + column, gates, 0.0), axis=1, keepdims=True)
        bias = jnp.sum(jnp.where(bias_lane == column, bias_ref[...], 0.0), axis=1, keepdims=True)
        pre = forget + bias
        log_forget = jnp.minimum(pre, 0.0) - jnp.log(1.0 + jnp.exp(-jnp.abs(pre)))
        old_m = jnp.sum(jnp.where(eye, m_ref[h : h + 1, :], 0.0), axis=1, keepdims=True)
        carried = log_forget + old_m
        new_m = jnp.maximum(carried, log_input)
        keep = jnp.exp(carried - new_m)
        admit = jnp.exp(log_input - new_m)
        newm_ref[h : h + 1, :] = jnp.sum(jnp.where(eye, new_m, 0.0), axis=0, keepdims=True)
        query = proj_ref[:, h * query_size : (h + 1) * query_size] * query_size ** (-0.5)
        key_at = query_width + h * query_size
        key = admit * proj_ref[:, key_at : key_at + query_size]
        v_at = value_at + h * value_size
        value = proj_ref[:, v_at : v_at + value_size]
        o_at = out_at + h * value_size
        out_pre = proj_ref[:, o_at : o_at + value_size]
        new_n = keep * n_ref[:, h, :] + key
        newn_ref[:, h, :] = new_n
        value_cols = value.T
        keep_wide = jnp.broadcast_to(keep, (rows, query_size))
        query_low = query.astype(jnp.bfloat16)
        read = jnp.zeros((rows, value_size), jnp.float32)
        for b in range(rows):
            loads[h * rows + b].wait()
            old = held[b, h]
            one = lax.dot_general(
                query_low, old.astype(jnp.bfloat16), (((1,), (1,)), ((), ())),
                preferred_element_type=jnp.float32,
            )
            read = jnp.where(sub == b, one, read)
            held[b, h] = (
                keep_wide[b : b + 1, :] * old + value_cols[:, b : b + 1] * key[b : b + 1, :]
            )
            store = pltpu.make_async_copy(held.at[b, h], newc_hbm.at[b, h], out_sem.at[b, h])
            store.start()
            stores.append(store)
        numer = keep * read + value * jnp.sum(key * query, axis=1, keepdims=True)
        denom = jnp.maximum(
            jnp.abs(jnp.sum(new_n * query, axis=1, keepdims=True)), jnp.exp(-new_m)
        )
        gated = numer / ((1.0 + jnp.exp(-out_pre)) * denom)
        head_ref[:, h * value_size : (h + 1) * value_size] = gated.astype(jnp.bfloat16)
    for store in stores:
        store.wait()


def hidden_spans(hidden):
    wide = -(-hidden // (SPANS * LANES)) * LANES
    return [(at, min(wide, hidden - at)) for at in range(0, hidden, wide)]


def tp_total(buf, send_sem, recv_sem):
    tp = lax.axis_index("tp")
    count = lax.axis_size("tp")
    copies = []
    for step in range(1, count):
        copy = remote("tp", step, buf.at[tp], buf.at[tp], send_sem.at[step], recv_sem.at[step])
        copy.start()
        copies.append(copy)
    for copy in copies:
        copy.wait_recv()
    total = buf[0].astype(jnp.float32)
    for i in range(1, count):
        total += buf[i].astype(jnp.float32)
    return total, copies


def rest_kernel(
    head_ref, tok_ref, gain_ref, wo, wg, wu, wd,
    mixed_ref,
    wo_v, wg_v, wu_v, wd_v, heads_all, abuf, dbuf, gpart, gland, gboth, glast,
    upart, uland, uboth, ulast, spart, sland, hbuf,
    load_sem, hsend, hrecv, asend, arecv, dsend, drecv, ssend, srecv, esend, erecv, fsend, frecv,
    bsend, brecv, csend, crecv,
):
    kv = lax.axis_index("kv")
    tp = lax.axis_index("tp")
    count = lax.axis_size("kv")
    batch, width = tok_ref.shape
    rows = batch // count
    loads = [
        pltpu.make_async_copy(src, dst, load_sem.at[i])
        for i, (src, dst) in enumerate([(wo, wo_v), (wg, wg_v), (wu, wu_v), (wd, wd_v)])
    ]
    barrier = pltpu.get_barrier_semaphore()
    signal_peers(barrier, "kv")
    signal_peers(barrier, "tp")
    for load in loads:
        load.start()
    pl.semaphore_wait(barrier, count - 1 + lax.axis_size("tp") - 1)
    gone = []
    arrive = []
    for step in range(1, count):
        copy = remote(
            "kv", step, head_ref, heads_all.at[kv], hsend.at[step], hrecv.at[step]
        )
        copy.start()
        arrive.append(copy)
    gone += arrive
    heads_all[kv] = head_ref[...]
    loads[0].wait()
    for copy in arrive:
        copy.wait_recv()
    heads = heads_all[...].astype(jnp.float32).reshape(batch, -1).astype(jnp.bfloat16)
    abuf[tp] = jnp.dot(heads, wo_v[...], preferred_element_type=jnp.float32).astype(jnp.bfloat16)
    attn_mix, copies = tp_total(abuf, asend, arecv)
    gone += copies
    middle = (tok_ref[...].astype(jnp.float32) + attn_mix).astype(jnp.bfloat16)
    mid = middle.astype(jnp.float32)
    squares = jnp.sum(mid * mid, axis=1, keepdims=True)
    normed = (mid * gain_ref[...]).astype(jnp.bfloat16)
    spart[...] = jnp.broadcast_to(squares, (batch, LANES)).reshape(count, rows, LANES)
    square_copies = [
        send_to(
            peer_of("kv", step), spart.at[peer_of("kv", step)], sland.at[step],
            ssend.at[step], srecv.at[step],
        )
        for step in range(1, count)
    ]
    gone += square_copies
    hidden = wg_v.shape[0]
    spans = hidden_spans(hidden)
    groups = []
    for w, (weight, part, land, both, last) in enumerate(
        [(wg_v, gpart, gland, gboth, glast), (wu_v, upart, uland, uboth, ulast)]
    ):
        loads[w + 1].wait()
        for k, (at, wide) in enumerate(spans):
            for off, size in pieces(wide):
                out = lax.dot_general(
                    normed, weight[at + off : at + off + size, :], (((1,), (1,)), ((), ())),
                    preferred_element_type=jnp.float32,
                )
                put_part(part, out, at + off, size)
            i = w * len(spans) + k
            first = scatter_first(i, part, land, pl.ds(at, wide), esend, erecv)
            groups.append((i, first, part, land, both, last, at, wide))
            gone += first
    seconds = [scatter_second(*group, fsend, frecv) for group in groups]
    for second in seconds:
        gone += second
    for copy in square_copies:
        copy.wait_recv()
    total = spart[kv]
    for step in range(1, count):
        total += sland[step]
    scale = lax.rsqrt(total[:, :1] / (width * count) + norm_floor)
    outer_at, inner_at, outer, inner = place()
    for k, (at, wide) in enumerate(spans):
        gate = scatter_sum(seconds[k], gboth, glast, at, wide) * scale
        up = scatter_sum(seconds[k + len(spans)], uboth, ulast, at, wide) * scale
        hid = gate / (1.0 + jnp.exp(-gate)) * up
        hbuf[outer_at, inner_at, :, at : at + wide] = hid.astype(jnp.bfloat16)
    own = hbuf.at[outer_at, inner_at]
    along = [
        send_to(outer_peer(step)[1], own, own, bsend.at[step], brecv.at[step])
        for step in range(1, outer)
    ]
    across = []
    for far in range(outer):
        if far > 0:
            along[far - 1].wait_recv()
        block = hbuf.at[(outer_at + outer - far) % outer, inner_at]
        for step in range(1, inner):
            across.append(
                send_to(inner_peer(step)[1], block, block, csend.at[far, step], crecv.at[far, step])
            )
    arrive = across
    gone += along + across
    loads[3].wait()
    for copy in arrive:
        copy.wait_recv()
    hid = hbuf[...].astype(jnp.float32).reshape(batch, -1).astype(jnp.bfloat16)
    dbuf[tp] = jnp.dot(hid, wd_v[...], preferred_element_type=jnp.float32).astype(jnp.bfloat16)
    down, copies = tp_total(dbuf, dsend, drecv)
    gone += copies
    mixed_ref[...] = (mid + down).astype(jnp.bfloat16)
    for copy in gone:
        copy.wait_send()


def per_device(
    tokens,
    attn_gain,
    w_query,
    w_key,
    w_value,
    w_outgate,
    w_gates,
    forget_bias,
    state_c,
    state_n,
    state_m,
    w_output,
    mlp_gain,
    w_gateff,
    w_upff,
    w_downff,
):
    f32, bf16 = jnp.float32, jnp.bfloat16
    count = lax.axis_size("kv")
    tps = lax.axis_size("tp")
    batch, width = tokens.shape
    rows, heads_dev, value_size, query_size = state_c.shape
    projections = (w_query, w_key, w_value, w_outgate)
    proj_width = sum(w.shape[1] for w in projections)
    hidden = w_gateff.shape[1]
    value_width = heads_dev * value_size
    rest_weights = (w_output, w_gateff.T, w_upff.T, w_downff)
    inner = inner_size(count)
    outer = count // inner
    spans = len(hidden_spans(hidden))
    sem = pltpu.SemaphoreType.DMA
    struct = jax.ShapeDtypeStruct

    proj, gates = pl.pallas_call(
        project_kernel,
        out_shape=(
            struct((rows, proj_width), f32),
            struct((rows, LANES), f32),
        ),
        in_specs=[VMEM_SPEC] * 2 + [HBM_SPEC] * 5,
        out_specs=(VMEM_SPEC, VMEM_SPEC),
        scratch_shapes=[pltpu.VMEM(w.shape, bf16) for w in projections]
        + [
            pltpu.VMEM((w_gates.shape[1], width), bf16),
            pltpu.VMEM((inner, outer, rows, proj_width), bf16),
            pltpu.VMEM((inner, outer, rows, proj_width), bf16),
            pltpu.VMEM((outer, rows, proj_width), bf16),
            pltpu.VMEM((outer, rows, proj_width), bf16),
            pltpu.VMEM((count, rows, LANES), f32),
            pltpu.VMEM((count, rows, LANES), f32),
            sem((5,)),
            sem((4, inner)),
            sem((4, inner)),
            sem((4, outer)),
            sem((4, outer)),
            sem((count,)),
            sem((count,)),
        ],
        compiler_params=pltpu.CompilerParams(
            collective_id=0, has_side_effects=True,
            vmem_limit_bytes=VMEM_ALL - SLACK,
        ),
        name="project",
    )(tokens, attn_gain[None], w_query, w_key, w_value, w_outgate, w_gates.T)

    head_out, new_n, new_m, new_c = pl.pallas_call(
        state_kernel,
        out_shape=(
            struct((rows, value_width), bf16),
            struct(state_n.shape, f32),
            struct(state_m.T.shape, f32),
            struct(state_c.shape, f32),
        ),
        in_specs=[VMEM_SPEC] * 5 + [HBM_SPEC],
        out_specs=(VMEM_SPEC, VMEM_SPEC, VMEM_SPEC, HBM_SPEC),
        scratch_shapes=[
            pltpu.VMEM(state_c.shape, f32),
            sem((rows, heads_dev)),
            sem((rows, heads_dev)),
        ],
        compiler_params=pltpu.CompilerParams(vmem_limit_bytes=VMEM_ALL - SLACK),
        name="state",
    )(proj, gates, forget_bias[None], state_m.T, state_n, state_c)

    mixed = pl.pallas_call(
        rest_kernel,
        out_shape=struct((batch, width), bf16),
        in_specs=[VMEM_SPEC] * 3 + [HBM_SPEC] * 4,
        out_specs=VMEM_SPEC,
        scratch_shapes=[pltpu.VMEM(w.shape, bf16) for w in rest_weights]
        + [
            pltpu.VMEM((count, rows, value_width), bf16),
            pltpu.VMEM((tps, batch, width), bf16),
            pltpu.VMEM((tps, batch, width), bf16),
        ]
        + [
            pltpu.VMEM((inner, outer, rows, hidden), bf16),
            pltpu.VMEM((inner, outer, rows, hidden), bf16),
            pltpu.VMEM((outer, rows, hidden), bf16),
            pltpu.VMEM((outer, rows, hidden), bf16),
        ]
        * 2
        + [
            pltpu.VMEM((count, rows, LANES), f32),
            pltpu.VMEM((count, rows, LANES), f32),
            pltpu.VMEM((outer, inner, rows, hidden), bf16),
            sem((4,)),
            sem((count,)),
            sem((count,)),
            sem((tps,)),
            sem((tps,)),
            sem((tps,)),
            sem((tps,)),
            sem((count,)),
            sem((count,)),
            sem((2 * spans, inner)),
            sem((2 * spans, inner)),
            sem((2 * spans, outer)),
            sem((2 * spans, outer)),
            sem((outer,)),
            sem((outer,)),
            sem((outer, inner)),
            sem((outer, inner)),
        ],
        compiler_params=pltpu.CompilerParams(
            collective_id=1, has_side_effects=True, vmem_limit_bytes=VMEM_ALL - SLACK
        ),
        name="rest",
    )(head_out, tokens, mlp_gain[None], *rest_weights)
    return (mixed, new_c, new_n, new_m.T)


def solution(mesh):
    placed = (
        P(None, "kv"),
        P("kv"),
        P("kv", "tp"),
        P("kv", "tp"),
        P("kv", "tp"),
        P("kv", "tp"),
        P(),
        P(),
        P("kv", "tp", None, None),
        P("kv", "tp", None),
        P("kv", "tp"),
        P("tp", "kv"),
        P("kv"),
        P("kv", "tp"),
        P("kv", "tp"),
        P("tp", "kv"),
    )
    return jax.shard_map(
        per_device,
        mesh=mesh,
        in_specs=placed,
        out_specs=(P(None, "kv"), P("kv", "tp", None, None), P("kv", "tp", None), P("kv", "tp")),
        check_vma=False,
    )
```

profile of v0, /device:TPU:1, one launch (start us, length us, event | category | flops | bytes accessed | tf_op | source)
XLA Modules:
  0.0 68.2 jit_solution(4372757698793335108)
XLA Ops:
  0.6 15.0 %project.1 = (f32[8,3072]{1,0:T(8,128)}, f32[8,128]{1,0:T(8,128)}) custom-call(bf16[64,512]{1,0:T(8,128)(2,1)} %tok_ref.3, f32[1,512]{1,0:T(1,128)} %bitcast.11, bf16[512,512]{1,0:T(8,128)(2,1)} %wq.1, bf16[512,512]{1,0:T(8,128)(2,1)} %wk.1, bf16[512,1024]{1,0:T(8,128)(2,1)} %wv.1, bf16[512,1024]{1,0:T(8,128)(2,1)} %wo.2, bf16[16,4096]{1,0:T(8,128)(2,1)} %bitcast.10), custom_call_target="tpu_custom_call" | custom-call | tf_op jit(solution)/shard_map/project/pallas_call | solution.py:450
  15.6 8.2 %state.1 = (bf16[8,1024]{1,0:T(8,128)(2,1)}, f32[8,2,256]{2,1,0:T(2,128)}, f32[2,8]{1,0:T(2,128)}, f32[8,2,512,256]{3,2,1,0:T(8,128)}) custom-call(f32[8,3072]{1,0:T(8,128)} %get-tuple-element.10.proj_ref, f32[8,128]{1,0:T(8,128)} %get-tuple-element.11.gate_ref, f32[1,8]{1,0:T(1,128)} %bitcast.14, f32[2,8]{1,0:T(2,128)} %bitcast.13, f32[8,2,256]{2,1,0:T(2,128)} %n_ref.1, ...), custom_call_target="tpu_custom_call" | custom-call | tf_op jit(solution)/shard_map/state/pallas_call | solution.py:482
  23.8 42.9 %rest.1 = bf16[64,512]{1,0:T(8,128)(2,1)} custom-call(bf16[8,1024]{1,0:T(8,128)(2,1)} %get-tuple-element.12.head_ref, bf16[64,512]{1,0:T(8,128)(2,1)} %tok_ref.3, f32[1,512]{1,0:T(1,128)} %bitcast.12, bf16[1024,512]{1,0:T(8,128)(2,1)} %wo.3, bf16[2752,512]{1,0:T(8,128)(2,1)} %bitcast.8, bf16[2752,512]{1,0:T(8,128)(2,1)} %bitcast.9, bf16[2752,512]{1,0:T(8,128)(2,1)} %wd.1), custom_call_target="tpu_custom_call" | custom-call | tf_op jit(solution)/shard_map/rest/pallas_call | solution.py:501
  66.8 1.5 %copy.21 = bf16[64,512]{1,0:T(8,128)(2,1)} copy(bf16[64,512]{1,0:T(8,128)(2,1)} %rest.1) | data formatting | bytes 131072
where the time goes:
time: 68.5 us; the launch traced here: 68.2 us
  Pallas kernels  66.1 us (96%)
  local copies, waits for them, and re-layouts  1.47 us (2%)
    pallas_call x1, Pallas kernels, per_device(): pl.pallas_call(rest_kernel, out_shape=struct((batch, width), bf16), in_sp...  42.9 us
    pallas_call x1, Pallas kernels, per_device(): pl.pallas_call(project_kernel, out_shape=(struct((rows, proj_width), f32)...  15 us
    pallas_call x1, Pallas kernels, per_device(): pl.pallas_call(state_kernel, out_shape=(struct((rows, value_width), bf16)...  8.22 us
    unnamed x1, local copies, waits for them, and re-layouts  1.47 us

commit v1 on v0

v1 whole, which is shorter than its diff:
```python
import jax
import jax.numpy as jnp
from jax import lax
from jax.experimental import pallas as pl
from jax.experimental.pallas import tpu as pltpu
from jax.sharding import PartitionSpec as P

norm_floor = 1e-05
MESH = pl.DeviceIdType.MESH
LANES = 128
SPAN = 512
VMEM_ALL = 67043328
ROOM = 4 * 1024 * 1024
VMEM_SPEC = pl.BlockSpec(memory_space=pltpu.VMEM)
HBM_SPEC = pl.BlockSpec(memory_space=pltpu.HBM)
F32, BF16 = jnp.float32, jnp.bfloat16


def peer_of(axis, step):
    count = lax.axis_size(axis)
    return lax.rem(lax.axis_index(axis) + step, count)


def signal_peers(barrier, axis):
    for step in range(1, lax.axis_size(axis)):
        pl.semaphore_signal(
            barrier, inc=1, device_id={axis: peer_of(axis, step)}, device_id_type=MESH
        )


def inner_size(count):
    size = 1 << ((count.bit_length() - 1) // 2)
    return size if count % size == 0 else 1


def place():
    count = lax.axis_size("kv")
    inner = inner_size(count)
    kv = lax.axis_index("kv")
    return kv // inner, kv % inner, count // inner, inner


def inner_peer(step):
    outer_at, inner_at, _, inner = place()
    return (inner_at + step) % inner, outer_at * inner + (inner_at + step) % inner


def outer_peer(step):
    outer_at, inner_at, outer, inner = place()
    return (outer_at + step) % outer, ((outer_at + step) % outer) * inner + inner_at


def send_to(axis, device, src, dst, send_sem, recv_sem):
    copy = pltpu.make_async_remote_copy(
        src_ref=src,
        dst_ref=dst,
        send_sem=send_sem,
        recv_sem=recv_sem,
        device_id={axis: device},
        device_id_type=MESH,
    )
    copy.start()
    return copy


def put_part(part, out, at, size):
    inner, outer, rows, _ = part.shape
    split = out.reshape(outer, inner, rows, size).astype(part.dtype)
    for i in range(inner):
        part[i, :, :, at : at + size] = split[:, i]


class Scatter:
    def __init__(self, part, land, both, last, esend, erecv, fsend, frecv):
        self.part, self.land, self.both, self.last = part, land, both, last
        self.esend, self.erecv, self.fsend, self.frecv = esend, erecv, fsend, frecv
        self.gone = []

    def first(self):
        inner = self.part.shape[0]
        self.one = []
        for step in range(1, inner):
            at, device = inner_peer(step)
            self.one.append(
                send_to(
                    "kv", device, self.part.at[at], self.land.at[step],
                    self.esend.at[step], self.erecv.at[step],
                )
            )
        self.gone += self.one

    def second(self):
        _, inner_at, outer, inner = place()
        for copy in self.one:
            copy.wait_recv()
        acc = self.part[inner_at].astype(F32)
        for step in range(1, inner):
            acc += self.land[step].astype(F32)
        self.both[...] = acc.astype(self.both.dtype)
        self.two = []
        for step in range(1, outer):
            to, device = outer_peer(step)
            self.two.append(
                send_to(
                    "kv", device, self.both.at[to], self.last.at[step],
                    self.fsend.at[step], self.frecv.at[step],
                )
            )
        self.gone += self.two

    def total(self):
        outer_at, _, outer, _ = place()
        for copy in self.two:
            copy.wait_recv()
        acc = self.both[outer_at].astype(F32)
        for step in range(1, outer):
            acc += self.last[step].astype(F32)
        return acc


def scatter_scratch(inner, outer, rows, wide, dtype):
    sem = pltpu.SemaphoreType.DMA
    return [
        pltpu.VMEM((inner, outer, rows, wide), dtype),
        pltpu.VMEM((inner, outer, rows, wide), dtype),
        pltpu.VMEM((outer, rows, wide), dtype),
        pltpu.VMEM((outer, rows, wide), dtype),
        sem((inner,)),
        sem((inner,)),
        sem((outer,)),
        sem((outer,)),
    ]


class Gather:
    def __init__(self, buf, asend, arecv, bsend, brecv):
        self.buf = buf
        self.asend, self.arecv, self.bsend, self.brecv = asend, arecv, bsend, brecv
        self.gone = []

    def send(self):
        outer_at, inner_at, outer, inner = place()
        own = self.buf.at[outer_at, inner_at]
        self.along = []
        self.across = []
        for step in range(1, outer):
            self.along.append(
                send_to("kv", outer_peer(step)[1], own, own, self.asend.at[step], self.arecv.at[step])
            )
        self._across(0)
        self.gone += self.along

    def _across(self, far):
        outer_at, inner_at, outer, inner = place()
        block = self.buf.at[(outer_at + outer - far) % outer, inner_at]
        for step in range(1, inner):
            copy = send_to(
                "kv", inner_peer(step)[1], block, block, self.bsend.at[far, step], self.brecv.at[far, step]
            )
            self.across.append(copy)
            self.gone.append(copy)

    def relay(self):
        for far, copy in enumerate(self.along):
            copy.wait_recv()
            self._across(far + 1)

    def wait(self):
        for copy in self.across:
            copy.wait_recv()


def gather_scratch(inner, outer, rows, wide):
    sem = pltpu.SemaphoreType.DMA
    return [
        pltpu.VMEM((outer, inner, rows, wide), BF16),
        sem((outer,)),
        sem((outer,)),
        sem((outer, inner)),
        sem((outer, inner)),
    ]


def tp_total(buf, send_sem, recv_sem):
    tp = lax.axis_index("tp")
    count = lax.axis_size("tp")
    copies = [
        send_to("tp", peer_of("tp", step), buf.at[tp], buf.at[tp], send_sem.at[step], recv_sem.at[step])
        for step in range(1, count)
    ]
    for copy in copies:
        copy.wait_recv()
    total = buf[0].astype(F32)
    for i in range(1, count):
        total += buf[i].astype(F32)
    return total, copies


def padded(wide):
    return -(-wide // LANES) * LANES


def hidden_spans(hidden):
    return [(at, min(SPAN, hidden - at)) for at in range(0, hidden, SPAN)]


def ffn_order(spans):
    events = []
    for k in range(spans):
        events += [(3.4 + 1.25 * k, 0, k), (7.8 + 1.25 * k, 1, k), (12.0 + 1.25 * k, 2, k), (14.5 + 1.25 * k, 3, k)]
    return [(kind, k) for _, kind, k in sorted(events)]


def layer_kernel(heads, spans, *refs):
    (
        tok_hbm, gain1_hbm, wq, wk, wv, wo, wg, bias_hbm, m_hbm, n_hbm, c_hbm, wout, gain2_hbm, wgf, wuf, wdf,
        mixed_ref, newc_ref, newn_ref, newm_ref,
    ) = refs[:20]
    scratch = list(refs[20:])

    def take(n):
        got = scratch[:n]
        del scratch[:n]
        return got

    tok_v, gain1_v, wq_v, wk_v, wv_v, wo_v, wg_v, wout_v, wgf_v, wuf_v, wdf_v = take(11)
    bias_ref, m_ref, n_ref, gain2_ref = take(4)
    wload, cload, sload = take(3)
    gates_rs = Scatter(*take(8))
    proj_rs = [Scatter(*take(8)) for _ in range(2 + 2 * heads)]
    head_ag = [Gather(*take(5)) for _ in range(heads)]
    ffn_rs = [Scatter(*take(8)) for _ in spans]
    square_rs = Scatter(*take(8))
    ffn_ag = [Gather(*take(5)) for _ in spans]
    abuf, dbuf, mid_v, acc_v, cols_v, asend, arecv, dsend, drecv = take(9)

    kv = lax.axis_index("kv")
    tp = lax.axis_index("tp")
    count = lax.axis_size("kv")
    outer_at, inner_at, outer, inner = place()
    batch, width = tok_v.shape
    rows = batch // count
    _, _, value_size, query_size = newc_ref.shape
    heads_all = bias_ref.shape[1]
    gate_cols = wg_v.shape[0]

    barrier = pltpu.get_barrier_semaphore()
    signal_peers(barrier, "kv")
    signal_peers(barrier, "tp")
    chunks = [(wq, wq_v, 0, heads * query_size), (wk, wk_v, 0, heads * query_size)]
    for h in range(heads):
        chunks.append((wv, wv_v, h * value_size, value_size))
        chunks.append((wo, wo_v, h * value_size, value_size))
    early = [
        pltpu.make_async_copy(tok_hbm, tok_v, wload.at[0]),
        pltpu.make_async_copy(gain1_hbm, gain1_v, wload.at[1]),
        pltpu.make_async_copy(
            wg.at[:, pl.ds(pl.multiple_of(kv * width, LANES), width)], wg_v, wload.at[2]
        ),
    ]
    for load in early:
        load.start()
    small = [
        pltpu.make_async_copy(src, dst, sload.at[i])
        for i, (src, dst) in enumerate(
            [(bias_hbm, bias_ref), (m_hbm, m_ref), (n_hbm, n_ref), (gain2_hbm, gain2_ref)]
        )
    ]
    for load in small:
        load.start()
    loads = []
    for i, (src, dst, at, wide) in enumerate(chunks):
        load = pltpu.make_async_copy(
            src.at[:, pl.ds(at, wide)], dst.at[:, pl.ds(at, wide)], wload.at[7 + i]
        )
        load.start()
        loads.append(load)
    early[0].wait()
    early[1].wait()
    tok = tok_v[...].astype(F32)
    squares = jnp.sum(tok * tok, axis=1, keepdims=True)
    normed = (tok * gain1_v[...]).astype(BF16)
    ready = []
    for i, (_, dst, at, wide) in enumerate(chunks):
        loads[i].wait()
        out = jnp.dot(normed, dst[:, at : at + wide], preferred_element_type=F32)
        put_part(proj_rs[i].part, out, 0, wide)
        if i == 1:
            early[2].wait()
            gates = lax.dot_general(
                normed, wg_v[...], (((1,), (1,)), ((), ())), preferred_element_type=F32
            )
            put_part(gates_rs.part, jnp.broadcast_to(squares, (batch, LANES)), 0, LANES)
            put_part(gates_rs.part, gates, 0, gate_cols)
            pl.semaphore_wait(barrier, count - 1 + lax.axis_size("tp") - 1)
            proj_rs[0].first()
            gates_rs.first()
            proj_rs[1].first()
        elif i > 1:
            proj_rs[i].first()
    cloads = [
        [pltpu.make_async_copy(c_hbm.at[b, h], newc_ref.at[b, h], cload.at[b, h]) for b in range(rows)]
        for h in range(heads)
    ]
    for group in cloads:
        for load in group:
            load.start()
    late = [
        pltpu.make_async_copy(src, dst, wload.at[3 + i])
        for i, (src, dst) in enumerate([(wout, wout_v), (wgf, wgf_v), (wuf, wuf_v), (wdf, wdf_v)])
    ]
    for load in late:
        load.start()
    for load in small:
        load.wait()
    proj_rs[0].second()
    gates_rs.second()
    for rs in proj_rs[1:]:
        rs.second()

    scale_query = proj_rs[0].total()
    gate_sum = gates_rs.total()
    scale = lax.rsqrt(gate_sum[:, gate_cols : gate_cols + 1] / (width * count) + norm_floor)
    gates = gate_sum * scale
    query_all = scale_query * (scale * query_size ** (-0.5))
    query_low = query_all.astype(BF16)
    lane = lax.broadcasted_iota(jnp.int32, gates.shape, 1)
    bias_lane = lax.broadcasted_iota(jnp.int32, bias_ref.shape, 1)
    sub = lax.broadcasted_iota(jnp.int32, (rows, value_size), 0)
    eye = lax.broadcasted_iota(jnp.int32, (rows, rows), 0) == lax.broadcasted_iota(
        jnp.int32, (rows, rows), 1
    )
    keeps, admits, new_ms = [], [], []
    for h in range(heads):
        column = tp * heads + h
        log_input = jnp.sum(jnp.where(lane == column, gates, 0.0), axis=1, keepdims=True)
        forget = jnp.sum(jnp.where(lane == heads_all + column, gates, 0.0), axis=1, keepdims=True)
        bias = jnp.sum(jnp.where(bias_lane == column, bias_ref[...], 0.0), axis=1, keepdims=True)
        pre = forget + bias
        log_forget = jnp.minimum(pre, 0.0) - jnp.log(1.0 + jnp.exp(-jnp.abs(pre)))
        old_m = jnp.sum(jnp.where(eye, m_ref[h : h + 1, :], 0.0), axis=1, keepdims=True)
        carried = log_forget + old_m
        new_m = jnp.maximum(carried, log_input)
        keeps.append(jnp.exp(carried - new_m))
        admits.append(jnp.exp(log_input - new_m))
        new_ms.append(new_m)
        newm_ref[h : h + 1, :] = jnp.sum(jnp.where(eye, new_m, 0.0), axis=0, keepdims=True)
    reads = []
    for h in range(heads):
        read = jnp.zeros((rows, value_size), F32)
        low = query_low[:, h * query_size : (h + 1) * query_size]
        for b in range(rows):
            cloads[h][b].wait()
            one = lax.dot_general(
                low, newc_ref[b, h].astype(BF16), (((1,), (1,)), ((), ())), preferred_element_type=F32
            )
            read = jnp.where(sub == b, one, read)
        reads.append(read)
    key_all = proj_rs[1].total() * scale
    keys = []
    for h in range(heads):
        query = query_all[:, h * query_size : (h + 1) * query_size]
        key = admits[h] * key_all[:, h * query_size : (h + 1) * query_size]
        keys.append(key)
        new_n = keeps[h] * n_ref[:, h, :] + key
        newn_ref[:, h, :] = new_n
        denom = jnp.maximum(
            jnp.abs(jnp.sum(new_n * query, axis=1, keepdims=True)), jnp.exp(-new_ms[h])
        )
        value = proj_rs[2 + 2 * h].total() * scale
        numer = keeps[h] * reads[h] + value * jnp.sum(key * query, axis=1, keepdims=True)
        cols_v[h] = value.T
        out_pre = proj_rs[3 + 2 * h].total() * scale
        gated = numer / ((1.0 + jnp.exp(-out_pre)) * denom)
        head_ag[h].buf[outer_at, inner_at] = gated.astype(BF16)
        head_ag[h].send()
    for h in range(heads):
        keep_wide = jnp.broadcast_to(keeps[h], (rows, query_size))
        for b in range(rows):
            newc_ref[b, h] = (
                keep_wide[b : b + 1, :] * newc_ref[b, h] + cols_v[h, :, b : b + 1] * keys[h][b : b + 1, :]
            )
        if h == 0:
            for ag in head_ag:
                ag.relay()

    late[0].wait()
    attn = None
    for h in range(heads):
        head_ag[h].wait()
        block = head_ag[h].buf[...].astype(F32).reshape(batch, value_size).astype(BF16)
        one = jnp.dot(block, wout_v[h * value_size : (h + 1) * value_size, :], preferred_element_type=F32)
        attn = one if attn is None else attn + one
    abuf[tp] = attn.astype(BF16)
    attn_mix, gone = tp_total(abuf, asend, arecv)
    middle = (tok_v[...].astype(F32) + attn_mix).astype(BF16)
    mid_v[...] = middle
    mid = middle.astype(F32)
    squares = jnp.sum(mid * mid, axis=1, keepdims=True)
    normed = (mid * gain2_ref[...]).astype(BF16)
    put_part(square_rs.part, jnp.broadcast_to(squares, (batch, LANES)), 0, LANES)
    square_rs.first()
    late[1].wait()
    late[2].wait()
    for k, (at, wide) in enumerate(spans):
        half = padded(wide)
        for j, weight in enumerate([wgf_v, wuf_v]):
            out = lax.dot_general(
                normed, weight[at : at + wide, :], (((1,), (1,)), ((), ())), preferred_element_type=F32
            )
            put_part(ffn_rs[k].part, out, j * half, wide)
            if half > wide:
                fill = jnp.zeros((batch, half - wide), F32)
                put_part(ffn_rs[k].part, fill, j * half + wide, half - wide)
        ffn_rs[k].first()
    square_rs.second()
    late[3].wait()
    scale2 = None
    for kind, k in ffn_order(len(spans)):
        at, wide = spans[k]
        half = padded(wide)
        if kind == 0:
            ffn_rs[k].second()
        elif kind == 1:
            if scale2 is None:
                total = square_rs.total()
                scale2 = lax.rsqrt(total[:, :1] / (width * count) + norm_floor)
            both = ffn_rs[k].total() * scale2
            gate = both[:, :wide]
            up = both[:, half : half + wide]
            hid = gate / (1.0 + jnp.exp(-gate)) * up
            ffn_ag[k].buf[outer_at, inner_at] = hid.astype(BF16)
            ffn_ag[k].send()
        elif kind == 2:
            ffn_ag[k].relay()
        else:
            ffn_ag[k].wait()
            hid = ffn_ag[k].buf[...].astype(F32).reshape(batch, wide).astype(BF16)
            one = jnp.dot(hid, wdf_v[at : at + wide, :], preferred_element_type=F32)
            if k == 0:
                acc_v[...] = one
            else:
                acc_v[...] += one
    dbuf[tp] = acc_v[...].astype(BF16)
    down, copies = tp_total(dbuf, dsend, drecv)
    mixed_ref[...] = (mid_v[...].astype(F32) + down).astype(BF16)
    gone += copies
    for group in [gates_rs, *proj_rs, *head_ag, square_rs, *ffn_rs, *ffn_ag]:
        gone += group.gone
    for copy in gone:
        copy.wait_send()


def store_kernel(mixed_in, c_in, n_in, m_in, mixed_out, c_out, n_out, m_out, sems):
    rows = c_in.shape[0]
    copies = [pltpu.make_async_copy(c_in.at[b], c_out.at[b], sems.at[b]) for b in range(rows)]
    copies += [
        pltpu.make_async_copy(src, dst, sems.at[rows + i])
        for i, (src, dst) in enumerate([(mixed_in, mixed_out), (n_in, n_out), (m_in, m_out)])
    ]
    for copy in copies:
        copy.start()
    for copy in copies:
        copy.wait()


def per_device(
    tokens,
    attn_gain,
    w_query,
    w_key,
    w_value,
    w_outgate,
    w_gates,
    forget_bias,
    state_c,
    state_n,
    state_m,
    w_output,
    mlp_gain,
    w_gateff,
    w_upff,
    w_downff,
):
    count = lax.axis_size("kv")
    tps = lax.axis_size("tp")
    batch, width = tokens.shape
    rows, heads, value_size, query_size = state_c.shape
    hidden = w_gateff.shape[1]
    inner = inner_size(count)
    outer = count // inner
    spans = hidden_spans(hidden)
    sem = pltpu.SemaphoreType.DMA
    struct = jax.ShapeDtypeStruct
    args = (
        tokens, attn_gain[None], w_query, w_key, w_value, w_outgate, w_gates.T,
        forget_bias[None], state_m.T, state_n, state_c, w_output, mlp_gain[None],
        w_gateff.T, w_upff.T, w_downff,
    )
    chunks = [heads * query_size] * 2 + [value_size] * (2 * heads)
    scratch = [
        pltpu.VMEM(tokens.shape, BF16),
        pltpu.VMEM((1, width), F32),
        *[pltpu.VMEM(w.shape, BF16) for w in (w_query, w_key, w_value, w_outgate)],
        pltpu.VMEM((w_gates.shape[1], width), BF16),
        *[pltpu.VMEM(w.shape, BF16) for w in (w_output, w_gateff.T, w_upff.T, w_downff)],
        *[pltpu.VMEM(args[i].shape, F32) for i in (7, 8, 9, 12)],
        sem((7 + len(chunks),)),
        sem((rows, heads)),
        sem((4,)),
    ]
    scratch += scatter_scratch(inner, outer, rows, LANES, F32)
    for wide in chunks:
        scratch += scatter_scratch(inner, outer, rows, wide, BF16)
    for _ in range(heads):
        scratch += gather_scratch(inner, outer, rows, value_size)
    for _, wide in spans:
        scratch += scatter_scratch(inner, outer, rows, 2 * padded(wide), BF16)
    scratch += scatter_scratch(inner, outer, rows, LANES, F32)
    for _, wide in spans:
        scratch += gather_scratch(inner, outer, rows, wide)
    scratch += [
        pltpu.VMEM((tps, batch, width), BF16),
        pltpu.VMEM((tps, batch, width), BF16),
        pltpu.VMEM((batch, width), BF16),
        pltpu.VMEM((batch, width), F32),
        pltpu.VMEM((heads, value_size, rows), F32),
        *[sem((tps,))] * 4,
    ]

    def kernel(*refs):
        layer_kernel(heads, spans, *refs)

    kernel_outs = (
        struct((batch, width), BF16),
        struct(state_c.shape, F32),
        struct(state_n.shape, F32),
        struct(state_m.T.shape, F32),
    )
    state_bytes = state_c.size * 4
    outs = pl.pallas_call(
        kernel,
        out_shape=kernel_outs,
        in_specs=[HBM_SPEC] * len(args),
        out_specs=(VMEM_SPEC,) * 4,
        scratch_shapes=scratch,
        compiler_params=pltpu.CompilerParams(
            collective_id=0, has_side_effects=True,
            vmem_limit_bytes=VMEM_ALL - state_bytes - ROOM,
        ),
        name="layer",
    )(*[pltpu.with_memory_space_constraint(arg, pltpu.HBM) for arg in args])
    mixed, new_c, new_n, new_m = pl.pallas_call(
        store_kernel,
        out_shape=kernel_outs,
        in_specs=[VMEM_SPEC] * 4,
        out_specs=(HBM_SPEC,) * 4,
        scratch_shapes=[sem((rows + 3,))],
        compiler_params=pltpu.CompilerParams(vmem_limit_bytes=ROOM),
        name="store",
    )(*outs)
    return (mixed, new_c, new_n, new_m.T)


def solution(mesh):
    placed = (
        P(None, "kv"),
        P("kv"),
        P("kv", "tp"),
        P("kv", "tp"),
        P("kv", "tp"),
        P("kv", "tp"),
        P(),
        P(),
        P("kv", "tp", None, None),
        P("kv", "tp", None),
        P("kv", "tp"),
        P("tp", "kv"),
        P("kv"),
        P("kv", "tp"),
        P("kv", "tp"),
        P("tp", "kv"),
    )
    return jax.shard_map(
        per_device,
        mesh=mesh,
        in_specs=placed,
        out_specs=(P(None, "kv"), P("kv", "tp", None, None), P("kv", "tp", None), P("kv", "tp")),
        check_vma=False,
    )
```

time: 68.5 us -> 68.6 us (level)
  local copies, waits for them, and re-layouts: 1.47 us -> 3.37 us
  Pallas kernels: 66.1 us -> 64.4 us
    unnamed x1 -> x2, local copies, waits for them, and re-layouts: 1.47 us -> 3.37 us
    pallas_call x3 -> x2, Pallas kernels: 66.1 us -> 64.4 us  [the longest x1 61 us: per_device(): pl.pallas_call(kernel, out_shape=kernel_outs, in_specs=[HBM_SPEC] * len(a...]
where the time goes in v1:
time: 68.6 us; the launch traced here: 68.4 us
  Pallas kernels  64.4 us (94%)
  local copies, waits for them, and re-layouts  3.37 us (5%)
    pallas_call x1, Pallas kernels, per_device(): pl.pallas_call(kernel, out_shape=kernel_outs, in_specs=[HBM_SPEC] * len(a...  61 us
    pallas_call x1, Pallas kernels, per_device(): pl.pallas_call(store_kernel, out_shape=kernel_outs, in_specs=[VMEM_SPEC]...  3.4 us
    unnamed x2, local copies, waits for them, and re-layouts  3.37 us

profile of v1, /device:TPU:1, one launch (start us, length us, event | category | flops | bytes accessed | tf_op | source)
XLA Modules:
  0.0 68.4 jit_solution(16096490687986834940)
XLA Ops:
  0.6 61.0 %layer.1 = (bf16[64,512]{1,0:T(8,128)(2,1)S(1)}, f32[8,2,512,256]{3,2,1,0:T(8,128)}, f32[8,2,256]{2,1,0:T(2,128)S(1)}, f32[2,8]{1,0:T(2,128)S(1)}) custom-call(bf16[64,512]{1,0:T(8,128)(2,1)} %refs_0_.1, f32[1,512]{1,0:T(1,128)} %bitcast.11, bf16[512,512]{1,0:T(8,128)(2,1)} %refs_2_.1, bf16[512,512]{1,0:T(8,128)(2,1)} %refs_3_.1, bf16[512,1024]{1,0:T(8,128)(2,1)} %refs_4_.1, ...), custom_call_target="tpu_custom_call" | custom-call | tf_op jit(solution)/shard_map/layer/pallas_call | solution.py:541
  61.7 0.0 copy-start
  61.7 3.4 %copy-done = f32[8,2,512,256]{3,2,1,0:T(8,128)S(1)} copy-done((f32[8,2,512,256]{3,2,1,0:T(8,128)S(1)}, f32[8,2,512,256]{3,2,1,0:T(8,128)}, u32[]{:S(2)}) %copy-start) | copy-done | bytes 8388632
  65.0 3.4 %store.1 = (bf16[64,512]{1,0:T(8,128)(2,1)}, f32[8,2,512,256]{3,2,1,0:T(8,128)}, f32[8,2,256]{2,1,0:T(2,128)}, f32[2,8]{1,0:T(2,128)}) custom-call(bf16[64,512]{1,0:T(8,128)(2,1)S(1)} %get-tuple-element.12.mixed_in, f32[8,2,512,256]{3,2,1,0:T(8,128)S(1)} %copy-done, f32[8,2,256]{2,1,0:T(2,128)S(1)} %get-tuple-element.14.n_in, f32[2,8]{1,0:T(2,128)S(1)} %get-tuple-element.15.m_in), custom_call_target="tpu_custom_call" | custom-call | tf_op jit(solution)/shard_map/store/pallas_call | solution.py:553
Async XLA Ops:
  61.7 3.4 %copy-start = (f32[8,2,512,256]{3,2,1,0:T(8,128)S(1)}, f32[8,2,512,256]{3,2,1,0:T(8,128)}, u32[]{:S(2)}) copy-start(f32[8,2,512,256]{3,2,1,0:T(8,128)} %get-tuple-element.13.c_in) | copy-start | bytes 25165828

commit v2 on v1

--- a/solution.py
+++ b/solution.py
@@ -9,6 +9,8 @@
 MESH = pl.DeviceIdType.MESH
 LANES = 128
 SPAN = 512
+EDGE = 256
+WINDOW = 3
 VMEM_ALL = 67043328
 ROOM = 4 * 1024 * 1024
 VMEM_SPEC = pl.BlockSpec(memory_space=pltpu.VMEM)
@@ -50,8 +52,8 @@
     return (outer_at + step) % outer, ((outer_at + step) % outer) * inner + inner_at
 
 
-def send_to(axis, device, src, dst, send_sem, recv_sem):
-    copy = pltpu.make_async_remote_copy(
+def remote_copy(axis, device, src, dst, send_sem, recv_sem):
+    return pltpu.make_async_remote_copy(
         src_ref=src,
         dst_ref=dst,
         send_sem=send_sem,
@@ -59,6 +61,10 @@
         device_id={axis: device},
         device_id_type=MESH,
     )
+
+
+def send_to(axis, device, src, dst, send_sem, recv_sem):
+    copy = remote_copy(axis, device, src, dst, send_sem, recv_sem)
     copy.start()
     return copy
 
@@ -76,22 +82,21 @@
         self.esend, self.erecv, self.fsend, self.frecv = esend, erecv, fsend, frecv
         self.gone = []
 
-    def first(self):
-        inner = self.part.shape[0]
-        self.one = []
-        for step in range(1, inner):
+    def one(self):
+        copies = []
+        for step in range(1, self.part.shape[0]):
             at, device = inner_peer(step)
-            self.one.append(
-                send_to(
+            copies.append(
+                remote_copy(
                     "kv", device, self.part.at[at], self.land.at[step],
                     self.esend.at[step], self.erecv.at[step],
                 )
             )
-        self.gone += self.one
+        return copies
 
     def second(self):
         _, inner_at, outer, inner = place()
-        for copy in self.one:
+        for copy in self.one():
             copy.wait_recv()
         acc = self.part[inner_at].astype(F32)
         for step in range(1, inner):
@@ -196,18 +201,69 @@
     return total, copies
 
 
+class Queue:
+    def __init__(self, scatters, turn):
+        self.scatters, self.turn = scatters, turn
+        self.tp = lax.axis_index("tp")
+        self.paired = lax.axis_size("tp") % 2 == 0
+
+    def _issue(self, k):
+        if k >= WINDOW:
+            for copy in self.scatters[k - WINDOW].one():
+                copy.wait_send()
+        for copy in self.scatters[k].one():
+            copy.start()
+
+    def early(self, k):
+        if not self.paired:
+            self._issue(k)
+            return
+
+        @pl.when(self.tp % 2 == 0)
+        def _():
+            self._issue(k)
+            if k == max(len(self.scatters) - 2, 0):
+                pl.semaphore_signal(self.turn, inc=1, device_id={"tp": self.tp + 1}, device_id_type=MESH)
+
+    def late(self):
+        if not self.paired:
+            return
+
+        @pl.when(self.tp % 2 == 1)
+        def _():
+            pl.semaphore_wait(self.turn, 1)
+            for k in range(len(self.scatters)):
+                self._issue(k)
+
+    def finish(self):
+        for scatter in self.scatters[-WINDOW:]:
+            for copy in scatter.one():
+                copy.wait_send()
+
+
 def padded(wide):
     return -(-wide // LANES) * LANES
 
 
 def hidden_spans(hidden):
-    return [(at, min(SPAN, hidden - at)) for at in range(0, hidden, SPAN)]
+    sizes = [min(EDGE, hidden)]
+    while hidden - sum(sizes) >= SPAN + EDGE:
+        sizes.append(SPAN)
+    while hidden > sum(sizes):
+        sizes.append(min(EDGE, hidden - sum(sizes)))
+    return [(sum(sizes[:k]), wide) for k, wide in enumerate(sizes)]
 
 
 def ffn_order(spans):
+    hidden = spans[-1][0] + spans[-1][1]
     events = []
-    for k in range(spans):
-        events += [(3.4 + 1.25 * k, 0, k), (7.8 + 1.25 * k, 1, k), (12.0 + 1.25 * k, 2, k), (14.5 + 1.25 * k, 3, k)]
+    for k, (at, wide) in enumerate(spans):
+        sent = 4.0 * (at + wide) / hidden
+        own = 4.0 * wide / hidden
+        second = sent + 2.6
+        total = second + 4.0 + own
+        relay = total + 4.0 + own / 2
+        events += [(at / hidden, 0, k), (second, 1, k), (total, 2, k), (relay, 3, k), (relay + 2.6 + own / 2, 4, k)]
     return [(kind, k) for _, kind, k in sorted(events)]
 
 
@@ -224,7 +280,7 @@
         return got
 
     tok_v, gain1_v, wq_v, wk_v, wv_v, wo_v, wg_v, wout_v, wgf_v, wuf_v, wdf_v = take(11)
-    bias_ref, m_ref, n_ref, gain2_ref = take(4)
+    bias_ref, m_ref, n_ref, gain2_ref, clow = take(5)
     wload, cload, sload = take(3)
     gates_rs = Scatter(*take(8))
     proj_rs = [Scatter(*take(8)) for _ in range(2 + 2 * heads)]
@@ -232,7 +288,7 @@
     ffn_rs = [Scatter(*take(8)) for _ in spans]
     square_rs = Scatter(*take(8))
     ffn_ag = [Gather(*take(5)) for _ in spans]
-    abuf, dbuf, mid_v, acc_v, cols_v, asend, arecv, dsend, drecv = take(9)
+    abuf, dbuf, mid_v, acc_v, cols_v, asend, arecv, dsend, drecv, turn = take(10)
 
     kv = lax.axis_index("kv")
     tp = lax.axis_index("tp")
@@ -280,9 +336,23 @@
     tok = tok_v[...].astype(F32)
     squares = jnp.sum(tok * tok, axis=1, keepdims=True)
     normed = (tok * gain1_v[...]).astype(BF16)
-    ready = []
+    proj_queue = Queue([proj_rs[0], gates_rs, *proj_rs[1:]], turn.at[0])
+    for load in loads:
+        load.wait()
+    cloads = [
+        [pltpu.make_async_copy(c_hbm.at[b, h], newc_ref.at[b, h], cload.at[b, h]) for b in range(rows)]
+        for h in range(heads)
+    ]
+    for group in cloads:
+        for load in group:
+            load.start()
+    late = [
+        pltpu.make_async_copy(src, dst, wload.at[3 + i])
+        for i, (src, dst) in enumerate([(wout, wout_v), (wgf, wgf_v), (wuf, wuf_v), (wdf, wdf_v)])
+    ]
+    for load in late:
+        load.start()
     for i, (_, dst, at, wide) in enumerate(chunks):
-        loads[i].wait()
         out = jnp.dot(normed, dst[:, at : at + wide], preferred_element_type=F32)
         put_part(proj_rs[i].part, out, 0, wide)
         if i == 1:
@@ -293,24 +363,11 @@
             put_part(gates_rs.part, jnp.broadcast_to(squares, (batch, LANES)), 0, LANES)
             put_part(gates_rs.part, gates, 0, gate_cols)
             pl.semaphore_wait(barrier, count - 1 + lax.axis_size("tp") - 1)
-            proj_rs[0].first()
-            gates_rs.first()
-            proj_rs[1].first()
+            for j in range(3):
+                proj_queue.early(j)
         elif i > 1:
-            proj_rs[i].first()
-    cloads = [
-        [pltpu.make_async_copy(c_hbm.at[b, h], newc_ref.at[b, h], cload.at[b, h]) for b in range(rows)]
-        for h in range(heads)
-    ]
-    for group in cloads:
-        for load in group:
-            load.start()
-    late = [
-        pltpu.make_async_copy(src, dst, wload.at[3 + i])
-        for i, (src, dst) in enumerate([(wout, wout_v), (wgf, wgf_v), (wuf, wuf_v), (wdf, wdf_v)])
-    ]
-    for load in late:
-        load.start()
+            proj_queue.early(i + 1)
+    proj_queue.late()
     for load in small:
         load.wait()
     proj_rs[0].second()
@@ -318,6 +375,12 @@
     for rs in proj_rs[1:]:
         rs.second()
 
+    for h in range(heads):
+        for b in range(rows):
+            cloads[h][b].wait()
+    for h in range(heads):
+        for b in range(rows):
+            clow[b, h] = newc_ref[b, h].astype(BF16)
     scale_query = proj_rs[0].total()
     gate_sum = gates_rs.total()
     scale = lax.rsqrt(gate_sum[:, gate_cols : gate_cols + 1] / (width * count) + norm_floor)
@@ -350,9 +413,8 @@
         read = jnp.zeros((rows, value_size), F32)
         low = query_low[:, h * query_size : (h + 1) * query_size]
         for b in range(rows):
-            cloads[h][b].wait()
             one = lax.dot_general(
-                low, newc_ref[b, h].astype(BF16), (((1,), (1,)), ((), ())), preferred_element_type=F32
+                low, clow[b, h], (((1,), (1,)), ((), ())), preferred_element_type=F32
             )
             read = jnp.where(sub == b, one, read)
         reads.append(read)
@@ -399,29 +461,32 @@
     squares = jnp.sum(mid * mid, axis=1, keepdims=True)
     normed = (mid * gain2_ref[...]).astype(BF16)
     put_part(square_rs.part, jnp.broadcast_to(squares, (batch, LANES)), 0, LANES)
-    square_rs.first()
     late[1].wait()
     late[2].wait()
-    for k, (at, wide) in enumerate(spans):
-        half = padded(wide)
-        for j, weight in enumerate([wgf_v, wuf_v]):
-            out = lax.dot_general(
-                normed, weight[at : at + wide, :], (((1,), (1,)), ((), ())), preferred_element_type=F32
-            )
-            put_part(ffn_rs[k].part, out, j * half, wide)
-            if half > wide:
-                fill = jnp.zeros((batch, half - wide), F32)
-                put_part(ffn_rs[k].part, fill, j * half + wide, half - wide)
-        ffn_rs[k].first()
-    square_rs.second()
-    late[3].wait()
+    ffn_queue = Queue([square_rs, *ffn_rs], turn.at[1])
     scale2 = None
-    for kind, k in ffn_order(len(spans)):
+    for kind, k in ffn_order(spans):
         at, wide = spans[k]
         half = padded(wide)
         if kind == 0:
+            for j, weight in enumerate([wgf_v, wuf_v]):
+                out = lax.dot_general(
+                    normed, weight[at : at + wide, :], (((1,), (1,)), ((), ())), preferred_element_type=F32
+                )
+                put_part(ffn_rs[k].part, out, j * half, wide)
+                if half > wide:
+                    fill = jnp.zeros((batch, half - wide), F32)
+                    put_part(ffn_rs[k].part, fill, j * half + wide, half - wide)
+            if k == 0:
+                ffn_queue.early(0)
+            ffn_queue.early(k + 1)
+            if k == len(spans) - 1:
+                ffn_queue.late()
+        elif kind == 1:
             ffn_rs[k].second()
-        elif kind == 1:
+            if k == 0:
+                square_rs.second()
+        elif kind == 2:
             if scale2 is None:
                 total = square_rs.total()
                 scale2 = lax.rsqrt(total[:, :1] / (width * count) + norm_floor)
@@ -431,10 +496,12 @@
             hid = gate / (1.0 + jnp.exp(-gate)) * up
             ffn_ag[k].buf[outer_at, inner_at] = hid.astype(BF16)
             ffn_ag[k].send()
-        elif kind == 2:
+        elif kind == 3:
             ffn_ag[k].relay()
         else:
             ffn_ag[k].wait()
+            if k == 0:
+                late[3].wait()
             hid = ffn_ag[k].buf[...].astype(F32).reshape(batch, wide).astype(BF16)
             one = jnp.dot(hid, wdf_v[at : at + wide, :], preferred_element_type=F32)
             if k == 0:
@@ -447,6 +514,8 @@
     gone += copies
     for group in [gates_rs, *proj_rs, *head_ag, square_rs, *ffn_rs, *ffn_ag]:
         gone += group.gone
+    proj_queue.finish()
+    ffn_queue.finish()
     for copy in gone:
         copy.wait_send()
 
@@ -505,6 +574,7 @@
         pltpu.VMEM((w_gates.shape[1], width), BF16),
         *[pltpu.VMEM(w.shape, BF16) for w in (w_output, w_gateff.T, w_upff.T, w_downff)],
         *[pltpu.VMEM(args[i].shape, F32) for i in (7, 8, 9, 12)],
+        pltpu.VMEM(state_c.shape, BF16),
         sem((7 + len(chunks),)),
         sem((rows, heads)),
         sem((4,)),
@@ -526,6 +596,7 @@
         pltpu.VMEM((batch, width), F32),
         pltpu.VMEM((heads, value_size, rows), F32),
         *[sem((tps,))] * 4,
+        pltpu.SemaphoreType.REGULAR((2,)),
     ]
 
     def kernel(*refs):
@@ -546,7 +617,7 @@
         scratch_shapes=scratch,
         compiler_params=pltpu.CompilerParams(
             collective_id=0, has_side_effects=True,
-            vmem_limit_bytes=VMEM_ALL - state_bytes - ROOM,
+            vmem_limit_bytes=VMEM_ALL - 3 * state_bytes,
         ),
         name="layer",
     )(*[pltpu.with_memory_space_constraint(arg, pltpu.HBM) for arg in args])

time: 68.6 us -> 60.2 us (0.88)
  Pallas kernels: 64.4 us -> 59.4 us
  local copies, waits for them, and re-layouts: 3.37 us -> 0 us
    pallas_call x1, Pallas kernels: 61 us -> 56 us  [per_device(): pl.pallas_call(kernel, out_shape=kernel_outs, in_specs=[HBM_SPEC] * len(a...]
    unnamed x2 -> x0, local copies, waits for them, and re-layouts: 3.37 us -> none
where the time goes in v2:
time: 60.2 us; the launch traced here: 60 us
  Pallas kernels  59.4 us (99%)
  between operations  0.65 us (1%)
    pallas_call x1, Pallas kernels, per_device(): pl.pallas_call(kernel, out_shape=kernel_outs, in_specs=[HBM_SPEC] * len(a...  56 us
    pallas_call x1, Pallas kernels, per_device(): pl.pallas_call(store_kernel, out_shape=kernel_outs, in_specs=[VMEM_SPEC]...  3.4 us

profile of v2, /device:TPU:1, one launch (start us, length us, event | category | flops | bytes accessed | tf_op | source)
XLA Modules:
  0.0 60.0 jit_solution(5877195351742909769)
XLA Ops:
  0.6 56.0 %layer.1 = (bf16[64,512]{1,0:T(8,128)(2,1)S(1)}, f32[8,2,512,256]{3,2,1,0:T(8,128)S(1)}, f32[8,2,256]{2,1,0:T(2,128)S(1)}, f32[2,8]{1,0:T(2,128)S(1)}) custom-call(bf16[64,512]{1,0:T(8,128)(2,1)} %refs_0_.1, f32[1,512]{1,0:T(1,128)} %bitcast.11, bf16[512,512]{1,0:T(8,128)(2,1)} %refs_2_.1, bf16[512,512]{1,0:T(8,128)(2,1)} %refs_3_.1, ...), custom_call_target="tpu_custom_call" | custom-call | tf_op jit(solution)/shard_map/layer/pallas_call | solution.py:612
  56.6 3.4 %store.1 = (bf16[64,512]{1,0:T(8,128)(2,1)}, f32[8,2,512,256]{3,2,1,0:T(8,128)}, f32[8,2,256]{2,1,0:T(2,128)}, f32[2,8]{1,0:T(2,128)}) custom-call(bf16[64,512]{1,0:T(8,128)(2,1)S(1)} %get-tuple-element.12.mixed_in, f32[8,2,512,256]{3,2,1,0:T(8,128)S(1)} %get-tuple-element.13.c_in, f32[8,2,256]{2,1,0:T(2,128)S(1)} %get-tuple-element.14.n_in, ...), custom_call_target="tpu_custom_call" | custom-call | tf_op jit(solution)/shard_map/store/pallas_call | solution.py:624

commit v3 on v2

--- a/solution.py
+++ b/solution.py
@@ -10,7 +10,8 @@
 LANES = 128
 SPAN = 512
 EDGE = 256
-WINDOW = 3
+PROJ_WINDOW, PROJ_HAND = 6, 2
+FFN_WINDOW, FFN_HAND = 3, 3
 VMEM_ALL = 67043328
 ROOM = 4 * 1024 * 1024
 VMEM_SPEC = pl.BlockSpec(memory_space=pltpu.VMEM)
@@ -63,12 +64,6 @@
     )
 
 
-def send_to(axis, device, src, dst, send_sem, recv_sem):
-    copy = remote_copy(axis, device, src, dst, send_sem, recv_sem)
-    copy.start()
-    return copy
-
-
 def put_part(part, out, at, size):
     inner, outer, rows, _ = part.shape
     split = out.reshape(outer, inner, rows, size).astype(part.dtype)
@@ -76,143 +71,126 @@
         part[i, :, :, at : at + size] = split[:, i]
 
 
+def wait_bytes(ref, sem):
+    pltpu.make_async_copy(ref, ref, sem).wait()
+
+
 class Scatter:
-    def __init__(self, part, land, both, last, esend, erecv, fsend, frecv):
+    def __init__(self, part, land, both, last, sems):
         self.part, self.land, self.both, self.last = part, land, both, last
-        self.esend, self.erecv, self.fsend, self.frecv = esend, erecv, fsend, frecv
-        self.gone = []
-
-    def one(self):
-        copies = []
+        self.sems = sems
+
+    def start(self):
         for step in range(1, self.part.shape[0]):
             at, device = inner_peer(step)
-            copies.append(
-                remote_copy(
-                    "kv", device, self.part.at[at], self.land.at[step],
-                    self.esend.at[step], self.erecv.at[step],
-                )
-            )
-        return copies
+            remote_copy(
+                "kv", device, self.part.at[at], self.land.at[step], self.sems.at[0], self.sems.at[1]
+            ).start()
+
+    def drain(self):
+        if self.part.shape[0] > 1:
+            wait_bytes(self.land.at[pl.ds(1, self.part.shape[0] - 1)], self.sems.at[0])
 
     def second(self):
         _, inner_at, outer, inner = place()
-        for copy in self.one():
-            copy.wait_recv()
+        if inner > 1:
+            wait_bytes(self.land.at[pl.ds(1, inner - 1)], self.sems.at[1])
         acc = self.part[inner_at].astype(F32)
         for step in range(1, inner):
             acc += self.land[step].astype(F32)
         self.both[...] = acc.astype(self.both.dtype)
-        self.two = []
         for step in range(1, outer):
             to, device = outer_peer(step)
-            self.two.append(
-                send_to(
-                    "kv", device, self.both.at[to], self.last.at[step],
-                    self.fsend.at[step], self.frecv.at[step],
-                )
-            )
-        self.gone += self.two
+            remote_copy(
+                "kv", device, self.both.at[to], self.last.at[step], self.sems.at[2], self.sems.at[3]
+            ).start()
 
     def total(self):
         outer_at, _, outer, _ = place()
-        for copy in self.two:
-            copy.wait_recv()
+        wait_bytes(self.last.at[pl.ds(1, outer - 1)], self.sems.at[3])
         acc = self.both[outer_at].astype(F32)
         for step in range(1, outer):
             acc += self.last[step].astype(F32)
         return acc
 
+    def settle(self):
+        wait_bytes(self.last.at[pl.ds(1, self.last.shape[0] - 1)], self.sems.at[2])
+
 
 def scatter_scratch(inner, outer, rows, wide, dtype):
-    sem = pltpu.SemaphoreType.DMA
     return [
         pltpu.VMEM((inner, outer, rows, wide), dtype),
         pltpu.VMEM((inner, outer, rows, wide), dtype),
         pltpu.VMEM((outer, rows, wide), dtype),
         pltpu.VMEM((outer, rows, wide), dtype),
-        sem((inner,)),
-        sem((inner,)),
-        sem((outer,)),
-        sem((outer,)),
+        pltpu.SemaphoreType.DMA((4,)),
     ]
 
 
 class Gather:
-    def __init__(self, buf, asend, arecv, bsend, brecv):
-        self.buf = buf
-        self.asend, self.arecv, self.bsend, self.brecv = asend, arecv, bsend, brecv
-        self.gone = []
-
-    def send(self):
-        outer_at, inner_at, outer, inner = place()
-        own = self.buf.at[outer_at, inner_at]
-        self.along = []
-        self.across = []
-        for step in range(1, outer):
-            self.along.append(
-                send_to("kv", outer_peer(step)[1], own, own, self.asend.at[step], self.arecv.at[step])
-            )
-        self._across(0)
-        self.gone += self.along
+    def __init__(self, buf, sems):
+        self.buf, self.sems = buf, sems
 
     def _across(self, far):
         outer_at, inner_at, outer, inner = place()
-        block = self.buf.at[(outer_at + outer - far) % outer, inner_at]
+        block = self.buf.at[(outer_at + outer - far) % outer * inner + inner_at]
         for step in range(1, inner):
-            copy = send_to(
-                "kv", inner_peer(step)[1], block, block, self.bsend.at[far, step], self.brecv.at[far, step]
-            )
-            self.across.append(copy)
-            self.gone.append(copy)
+            remote_copy("kv", inner_peer(step)[1], block, block, self.sems.at[0], self.sems.at[2]).start()
+
+    def send(self):
+        outer = place()[2]
+        own = self.buf.at[lax.axis_index("kv")]
+        for step in range(outer - 1, 0, -1):
+            remote_copy("kv", outer_peer(step)[1], own, own, self.sems.at[0], self.sems.at[1]).start()
+        self._across(0)
 
     def relay(self):
-        for far, copy in enumerate(self.along):
-            copy.wait_recv()
-            self._across(far + 1)
+        outer = place()[2]
+        wait_bytes(self.buf.at[pl.ds(1, outer - 1)], self.sems.at[1])
+        for far in range(1, outer):
+            self._across(far)
 
     def wait(self):
-        for copy in self.across:
-            copy.wait_recv()
-
-
-def gather_scratch(inner, outer, rows, wide):
-    sem = pltpu.SemaphoreType.DMA
-    return [
-        pltpu.VMEM((outer, inner, rows, wide), BF16),
-        sem((outer,)),
-        sem((outer,)),
-        sem((outer, inner)),
-        sem((outer, inner)),
-    ]
-
-
-def tp_total(buf, send_sem, recv_sem):
+        _, _, outer, inner = place()
+        if inner > 1:
+            wait_bytes(self.buf.at[pl.ds(0, outer * (inner - 1))], self.sems.at[2])
+
+    def settle(self):
+        wait_bytes(self.buf.at[pl.ds(1, self.buf.shape[0] - 1)], self.sems.at[0])
+
+
+def gather_scratch(count, rows, wide):
+    return [pltpu.VMEM((count, rows, wide), BF16), pltpu.SemaphoreType.DMA((3,))]
+
+
+def tp_send(buf, sems):
     tp = lax.axis_index("tp")
-    count = lax.axis_size("tp")
-    copies = [
-        send_to("tp", peer_of("tp", step), buf.at[tp], buf.at[tp], send_sem.at[step], recv_sem.at[step])
-        for step in range(1, count)
-    ]
-    for copy in copies:
-        copy.wait_recv()
+    for step in range(1, buf.shape[0]):
+        remote_copy("tp", peer_of("tp", step), buf.at[tp], buf.at[tp], sems.at[0], sems.at[1]).start()
+
+
+def tp_total(buf, sems):
+    wait_bytes(buf.at[pl.ds(1, buf.shape[0] - 1)], sems.at[1])
     total = buf[0].astype(F32)
-    for i in range(1, count):
+    for i in range(1, buf.shape[0]):
         total += buf[i].astype(F32)
-    return total, copies
+    return total
+
+
+def tp_settle(buf, sems):
+    wait_bytes(buf.at[pl.ds(1, buf.shape[0] - 1)], sems.at[0])
 
 
 class Queue:
-    def __init__(self, scatters, turn):
-        self.scatters, self.turn = scatters, turn
+    def __init__(self, scatters, turn, window, hand):
+        self.scatters, self.turn, self.window, self.hand = scatters, turn, window, max(len(scatters) - hand, 0)
         self.tp = lax.axis_index("tp")
         self.paired = lax.axis_size("tp") % 2 == 0
 
     def _issue(self, k):
-        if k >= WINDOW:
-            for copy in self.scatters[k - WINDOW].one():
-                copy.wait_send()
-        for copy in self.scatters[k].one():
-            copy.start()
+        if k >= self.window:
+            self.scatters[k - self.window].drain()
+        self.scatters[k].start()
 
     def early(self, k):
         if not self.paired:
@@ -222,7 +200,7 @@
         @pl.when(self.tp % 2 == 0)
         def _():
             self._issue(k)
-            if k == max(len(self.scatters) - 2, 0):
+            if k == self.hand:
                 pl.semaphore_signal(self.turn, inc=1, device_id={"tp": self.tp + 1}, device_id_type=MESH)
 
     def late(self):
@@ -236,9 +214,8 @@
                 self._issue(k)
 
     def finish(self):
-        for scatter in self.scatters[-WINDOW:]:
-            for copy in scatter.one():
-                copy.wait_send()
+        for scatter in self.scatters[-self.window :]:
+            scatter.drain()
 
 
 def padded(wide):
@@ -282,13 +259,13 @@
     tok_v, gain1_v, wq_v, wk_v, wv_v, wo_v, wg_v, wout_v, wgf_v, wuf_v, wdf_v = take(11)
     bias_ref, m_ref, n_ref, gain2_ref, clow = take(5)
     wload, cload, sload = take(3)
-    gates_rs = Scatter(*take(8))
-    proj_rs = [Scatter(*take(8)) for _ in range(2 + 2 * heads)]
-    head_ag = [Gather(*take(5)) for _ in range(heads)]
-    ffn_rs = [Scatter(*take(8)) for _ in spans]
-    square_rs = Scatter(*take(8))
-    ffn_ag = [Gather(*take(5)) for _ in spans]
-    abuf, dbuf, mid_v, acc_v, cols_v, asend, arecv, dsend, drecv, turn = take(10)
+    gates_rs = Scatter(*take(5))
+    proj_rs = [Scatter(*take(5)) for _ in range(2 + 2 * heads)]
+    head_ag = [Gather(*take(2)) for _ in range(heads)]
+    ffn_rs = [Scatter(*take(5)) for _ in spans]
+    square_rs = Scatter(*take(5))
+    ffn_ag = [Gather(*take(2)) for _ in spans]
+    abuf, dbuf, mid_v, acc_v, cols_v, asem, dsem, turn = take(8)
 
     kv = lax.axis_index("kv")
     tp = lax.axis_index("tp")
@@ -334,38 +311,34 @@
     early[0].wait()
     early[1].wait()
     tok = tok_v[...].astype(F32)
-    squares = jnp.sum(tok * tok, axis=1, keepdims=True)
     normed = (tok * gain1_v[...]).astype(BF16)
-    proj_queue = Queue([proj_rs[0], gates_rs, *proj_rs[1:]], turn.at[0])
-    for load in loads:
-        load.wait()
-    cloads = [
-        [pltpu.make_async_copy(c_hbm.at[b, h], newc_ref.at[b, h], cload.at[b, h]) for b in range(rows)]
-        for h in range(heads)
-    ]
-    for group in cloads:
-        for load in group:
-            load.start()
-    late = [
-        pltpu.make_async_copy(src, dst, wload.at[3 + i])
-        for i, (src, dst) in enumerate([(wout, wout_v), (wgf, wgf_v), (wuf, wuf_v), (wdf, wdf_v)])
-    ]
-    for load in late:
-        load.start()
+    proj_queue = Queue([proj_rs[0], gates_rs, *proj_rs[1:]], turn.at[0], PROJ_WINDOW, PROJ_HAND)
     for i, (_, dst, at, wide) in enumerate(chunks):
+        loads[i].wait()
+        if i == len(chunks) - 1:
+            for h in range(heads):
+                for b in range(rows):
+                    pltpu.make_async_copy(c_hbm.at[b, h], newc_ref.at[b, h], cload).start()
+            late = [
+                pltpu.make_async_copy(src, dst, wload.at[3 + i])
+                for i, (src, dst) in enumerate([(wout, wout_v), (wgf, wgf_v), (wuf, wuf_v), (wdf, wdf_v)])
+            ]
+            for load in late:
+                load.start()
         out = jnp.dot(normed, dst[:, at : at + wide], preferred_element_type=F32)
         put_part(proj_rs[i].part, out, 0, wide)
-        if i == 1:
+        if i == 0:
+            pl.semaphore_wait(barrier, count - 1 + lax.axis_size("tp") - 1)
+            proj_queue.early(0)
             early[2].wait()
             gates = lax.dot_general(
                 normed, wg_v[...], (((1,), (1,)), ((), ())), preferred_element_type=F32
             )
+            squares = jnp.sum(tok * tok, axis=1, keepdims=True)
             put_part(gates_rs.part, jnp.broadcast_to(squares, (batch, LANES)), 0, LANES)
             put_part(gates_rs.part, gates, 0, gate_cols)
-            pl.semaphore_wait(barrier, count - 1 + lax.axis_size("tp") - 1)
-            for j in range(3):
-                proj_queue.early(j)
-        elif i > 1:
+            proj_queue.early(1)
+        else:
             proj_queue.early(i + 1)
     proj_queue.late()
     for load in small:
@@ -375,9 +348,7 @@
     for rs in proj_rs[1:]:
         rs.second()
 
-    for h in range(heads):
-        for b in range(rows):
-            cloads[h][b].wait()
+    wait_bytes(newc_ref, cload)
     for h in range(heads):
         for b in range(rows):
             clow[b, h] = newc_ref[b, h].astype(BF16)
@@ -434,7 +405,7 @@
         cols_v[h] = value.T
         out_pre = proj_rs[3 + 2 * h].total() * scale
         gated = numer / ((1.0 + jnp.exp(-out_pre)) * denom)
-        head_ag[h].buf[outer_at, inner_at] = gated.astype(BF16)
+        head_ag[h].buf[kv] = gated.astype(BF16)
         head_ag[h].send()
     for h in range(heads):
         keep_wide = jnp.broadcast_to(keeps[h], (rows, query_size))
@@ -454,7 +425,11 @@
         one = jnp.dot(block, wout_v[h * value_size : (h + 1) * value_size, :], preferred_element_type=F32)
         attn = one if attn is None else attn + one
     abuf[tp] = attn.astype(BF16)
-    attn_mix, gone = tp_total(abuf, asend, arecv)
+    tp_send(abuf, asem)
+    for group in [gates_rs, *proj_rs, *head_ag]:
+        group.settle()
+    proj_queue.finish()
+    attn_mix = tp_total(abuf, asem)
     middle = (tok_v[...].astype(F32) + attn_mix).astype(BF16)
     mid_v[...] = middle
     mid = middle.astype(F32)
@@ -463,7 +438,7 @@
     put_part(square_rs.part, jnp.broadcast_to(squares, (batch, LANES)), 0, LANES)
     late[1].wait()
     late[2].wait()
-    ffn_queue = Queue([square_rs, *ffn_rs], turn.at[1])
+    ffn_queue = Queue([square_rs, *ffn_rs], turn.at[1], FFN_WINDOW, FFN_HAND)
     scale2 = None
     for kind, k in ffn_order(spans):
         at, wide = spans[k]
@@ -494,7 +469,7 @@
             gate = both[:, :wide]
             up = both[:, half : half + wide]
             hid = gate / (1.0 + jnp.exp(-gate)) * up
-            ffn_ag[k].buf[outer_at, inner_at] = hid.astype(BF16)
+            ffn_ag[k].buf[kv] = hid.astype(BF16)
             ffn_ag[k].send()
         elif kind == 3:
             ffn_ag[k].relay()
@@ -509,15 +484,14 @@
             else:
                 acc_v[...] += one
     dbuf[tp] = acc_v[...].astype(BF16)
-    down, copies = tp_total(dbuf, dsend, drecv)
+    tp_send(dbuf, dsem)
+    for group in [square_rs, *ffn_rs, *ffn_ag]:
+        group.settle()
+    ffn_queue.finish()
+    tp_settle(abuf, asem)
+    down = tp_total(dbuf, dsem)
     mixed_ref[...] = (mid_v[...].astype(F32) + down).astype(BF16)
-    gone += copies
-    for group in [gates_rs, *proj_rs, *head_ag, square_rs, *ffn_rs, *ffn_ag]:
-        gone += group.gone
-    proj_queue.finish()
-    ffn_queue.finish()
-    for copy in gone:
-        copy.wait_send()
+    tp_settle(dbuf, dsem)
 
 
 def store_kernel(mixed_in, c_in, n_in, m_in, mixed_out, c_out, n_out, m_out, sems):
@@ -576,26 +550,26 @@
         *[pltpu.VMEM(args[i].shape, F32) for i in (7, 8, 9, 12)],
         pltpu.VMEM(state_c.shape, BF16),
         sem((7 + len(chunks),)),
-        sem((rows, heads)),
+        sem,
         sem((4,)),
     ]
     scratch += scatter_scratch(inner, outer, rows, LANES, F32)
     for wide in chunks:
         scratch += scatter_scratch(inner, outer, rows, wide, BF16)
     for _ in range(heads):
-        scratch += gather_scratch(inner, outer, rows, value_size)
+        scratch += gather_scratch(count, rows, value_size)
     for _, wide in spans:
         scratch += scatter_scratch(inner, outer, rows, 2 * padded(wide), BF16)
     scratch += scatter_scratch(inner, outer, rows, LANES, F32)
     for _, wide in spans:
-        scratch += gather_scratch(inner, outer, rows, wide)
+        scratch += gather_scratch(count, rows, wide)
     scratch += [
         pltpu.VMEM((tps, batch, width), BF16),
         pltpu.VMEM((tps, batch, width), BF16),
         pltpu.VMEM((batch, width), BF16),
         pltpu.VMEM((batch, width), F32),
         pltpu.VMEM((heads, value_size, rows), F32),
-        *[sem((tps,))] * 4,
+        *[sem((2,))] * 2,
         pltpu.SemaphoreType.REGULAR((2,)),
     ]
 

time: 60.2 us -> 57.5 us (0.955)
  Pallas kernels: 59.4 us -> 56.7 us
    pallas_call x1, Pallas kernels: 56 us -> 53.3 us  [per_device(): pl.pallas_call(kernel, out_shape=kernel_outs, in_specs=[HBM_SPEC] * len(a...]
where the time goes in v3:
time: 57.5 us; the launch traced here: 57.4 us
  Pallas kernels  56.7 us (99%)
  between operations  0.65 us (1%)
    pallas_call x1, Pallas kernels, per_device(): pl.pallas_call(kernel, out_shape=kernel_outs, in_specs=[HBM_SPEC] * len(a...  53.3 us
    pallas_call x1, Pallas kernels, per_device(): pl.pallas_call(store_kernel, out_shape=kernel_outs, in_specs=[VMEM_SPEC]...  3.4 us

profile of v3, /device:TPU:1, one launch (start us, length us, event | category | flops | bytes accessed | tf_op | source)
XLA Modules:
  0.0 57.4 jit_solution(17309175876307738794)
XLA Ops:
  0.6 53.3 %layer.1 = (bf16[64,512]{1,0:T(8,128)(2,1)S(1)}, f32[8,2,512,256]{3,2,1,0:T(8,128)S(1)}, f32[8,2,256]{2,1,0:T(2,128)S(1)}, f32[2,8]{1,0:T(2,128)S(1)}) custom-call(bf16[64,512]{1,0:T(8,128)(2,1)} %refs_0_.1, f32[1,512]{1,0:T(1,128)} %bitcast.11, bf16[512,512]{1,0:T(8,128)(2,1)} %refs_2_.1, bf16[512,512]{1,0:T(8,128)(2,1)} %refs_3_.1, ...), custom_call_target="tpu_custom_call" | custom-call | tf_op jit(solution)/shard_map/layer/pallas_call | solution.py:586
  54.0 3.4 %store.1 = (bf16[64,512]{1,0:T(8,128)(2,1)}, f32[8,2,512,256]{3,2,1,0:T(8,128)}, f32[8,2,256]{2,1,0:T(2,128)}, f32[2,8]{1,0:T(2,128)}) custom-call(bf16[64,512]{1,0:T(8,128)(2,1)S(1)} %get-tuple-element.12.mixed_in, f32[8,2,512,256]{3,2,1,0:T(8,128)S(1)} %get-tuple-element.13.c_in, f32[8,2,256]{2,1,0:T(2,128)S(1)} %get-tuple-element.14.n_in, ...), custom_call_target="tpu_custom_call" | custom-call | tf_op jit(solution)/shard_map/store/pallas_call | solution.py:598

commit v4 on v3

--- a/solution.py
+++ b/solution.py
@@ -11,7 +11,9 @@
 SPAN = 512
 EDGE = 256
 PROJ_WINDOW, PROJ_HAND = 6, 2
-FFN_WINDOW, FFN_HAND = 3, 3
+FFN_WINDOW, FFN_HAND = 3, 1
+OUTER_SPAN, OUTER_AT = 640, (1,)
+
 VMEM_ALL = 67043328
 ROOM = 4 * 1024 * 1024
 VMEM_SPEC = pl.BlockSpec(memory_space=pltpu.VMEM)
@@ -64,91 +66,106 @@
     )
 
 
-def put_part(part, out, at, size):
-    inner, outer, rows, _ = part.shape
-    split = out.reshape(outer, inner, rows, size).astype(part.dtype)
-    for i in range(inner):
-        part[i, :, :, at : at + size] = split[:, i]
-
-
 def wait_bytes(ref, sem):
     pltpu.make_async_copy(ref, ref, sem).wait()
 
 
 class Scatter:
-    def __init__(self, part, land, both, last, sems):
+    def __init__(self, part, land, both, last, sems, inner_first=True):
         self.part, self.land, self.both, self.last = part, land, both, last
-        self.sems = sems
+        self.sems, self.inner_first = sems, inner_first
+        self.firsts, self.seconds = part.shape[0], part.shape[1]
+
+    def _peers(self):
+        return (inner_peer, outer_peer) if self.inner_first else (outer_peer, inner_peer)
+
+    def _places(self):
+        outer_at, inner_at, _, _ = place()
+        return (inner_at, outer_at) if self.inner_first else (outer_at, inner_at)
+
+    def put(self, out, at, size):
+        inner, outer = (self.firsts, self.seconds) if self.inner_first else (self.seconds, self.firsts)
+        split = out.reshape(outer, inner, self.part.shape[2], size).astype(self.part.dtype)
+        for i in range(self.firsts):
+            self.part[i, :, :, at : at + size] = split[:, i] if self.inner_first else split[i]
 
     def start(self):
-        for step in range(1, self.part.shape[0]):
-            at, device = inner_peer(step)
+        for step in range(self.firsts - 1, 0, -1):
+            at, device = self._peers()[0](step)
             remote_copy(
                 "kv", device, self.part.at[at], self.land.at[step], self.sems.at[0], self.sems.at[1]
             ).start()
 
     def drain(self):
-        if self.part.shape[0] > 1:
-            wait_bytes(self.land.at[pl.ds(1, self.part.shape[0] - 1)], self.sems.at[0])
+        if self.firsts > 1:
+            wait_bytes(self.land.at[pl.ds(1, self.firsts - 1)], self.sems.at[0])
 
     def second(self):
-        _, inner_at, outer, inner = place()
-        if inner > 1:
-            wait_bytes(self.land.at[pl.ds(1, inner - 1)], self.sems.at[1])
-        acc = self.part[inner_at].astype(F32)
-        for step in range(1, inner):
+        if self.firsts > 1:
+            wait_bytes(self.land.at[pl.ds(1, self.firsts - 1)], self.sems.at[1])
+        acc = self.part[self._places()[0]].astype(F32)
+        for step in range(1, self.firsts):
             acc += self.land[step].astype(F32)
         self.both[...] = acc.astype(self.both.dtype)
-        for step in range(1, outer):
-            to, device = outer_peer(step)
+        for step in range(1, self.seconds):
+            to, device = self._peers()[1](step)
             remote_copy(
                 "kv", device, self.both.at[to], self.last.at[step], self.sems.at[2], self.sems.at[3]
             ).start()
 
     def total(self):
-        outer_at, _, outer, _ = place()
-        wait_bytes(self.last.at[pl.ds(1, outer - 1)], self.sems.at[3])
-        acc = self.both[outer_at].astype(F32)
-        for step in range(1, outer):
+        if self.seconds > 1:
+            wait_bytes(self.last.at[pl.ds(1, self.seconds - 1)], self.sems.at[3])
+        acc = self.both[self._places()[1]].astype(F32)
+        for step in range(1, self.seconds):
             acc += self.last[step].astype(F32)
         return acc
 
     def settle(self):
-        wait_bytes(self.last.at[pl.ds(1, self.last.shape[0] - 1)], self.sems.at[2])
-
-
-def scatter_scratch(inner, outer, rows, wide, dtype):
+        if self.seconds > 1:
+            wait_bytes(self.last.at[pl.ds(1, self.seconds - 1)], self.sems.at[2])
+
+
+def scatter_scratch(firsts, seconds, rows, wide, dtype):
     return [
-        pltpu.VMEM((inner, outer, rows, wide), dtype),
-        pltpu.VMEM((inner, outer, rows, wide), dtype),
-        pltpu.VMEM((outer, rows, wide), dtype),
-        pltpu.VMEM((outer, rows, wide), dtype),
+        pltpu.VMEM((firsts, seconds, rows, wide), dtype),
+        pltpu.VMEM((firsts, seconds, rows, wide), dtype),
+        pltpu.VMEM((seconds, rows, wide), dtype),
+        pltpu.VMEM((seconds, rows, wide), dtype),
         pltpu.SemaphoreType.DMA((4,)),
     ]
 
 
 class Gather:
-    def __init__(self, buf, sems):
-        self.buf, self.sems = buf, sems
+    def __init__(self, buf, sems, direct=False):
+        self.buf, self.sems, self.direct = buf, sems, direct
+
+    def _send(self, device, block, sem):
+        block = self.buf.at[block]
+        remote_copy("kv", device, block, block, self.sems.at[0], self.sems.at[sem]).start()
 
     def _across(self, far):
         outer_at, inner_at, outer, inner = place()
-        block = self.buf.at[(outer_at + outer - far) % outer * inner + inner_at]
+        block = (outer_at + outer - far) % outer * inner + inner_at
         for step in range(1, inner):
-            remote_copy("kv", inner_peer(step)[1], block, block, self.sems.at[0], self.sems.at[2]).start()
+            self._send(inner_peer(step)[1], block, 2)
 
     def send(self):
-        outer = place()[2]
-        own = self.buf.at[lax.axis_index("kv")]
+        outer_at, inner_at, outer, inner = place()
+        own = lax.axis_index("kv")
         for step in range(outer - 1, 0, -1):
-            remote_copy("kv", outer_peer(step)[1], own, own, self.sems.at[0], self.sems.at[1]).start()
+            if self.direct:
+                for side in range(1, inner):
+                    self._send((outer_at + step) % outer * inner + (inner_at + side) % inner, own, 2)
+            self._send(outer_peer(step)[1], own, 1)
         self._across(0)
 
     def relay(self):
         outer = place()[2]
         wait_bytes(self.buf.at[pl.ds(1, outer - 1)], self.sems.at[1])
-        for far in range(1, outer):
-            self._across(far)
+        if not self.direct:
+            for far in range(1, outer):
+                self._across(far)
 
     def wait(self):
         _, _, outer, inner = place()
@@ -223,24 +240,29 @@
 
 
 def hidden_spans(hidden):
-    sizes = [min(EDGE, hidden)]
+    sizes = []
     while hidden - sum(sizes) >= SPAN + EDGE:
-        sizes.append(SPAN)
+        sizes.append(OUTER_SPAN if len(sizes) in OUTER_AT else SPAN)
     while hidden > sum(sizes):
         sizes.append(min(EDGE, hidden - sum(sizes)))
-    return [(sum(sizes[:k]), wide) for k, wide in enumerate(sizes)]
+    return [(sum(sizes[:k]), wide, k not in OUTER_AT) for k, wide in enumerate(sizes)]
 
 
 def ffn_order(spans):
     hidden = spans[-1][0] + spans[-1][1]
+    inner_sum = outer_sum = 0.0
     events = []
-    for k, (at, wide) in enumerate(spans):
-        sent = 4.0 * (at + wide) / hidden
-        own = 4.0 * wide / hidden
-        second = sent + 2.6
-        total = second + 4.0 + own
-        relay = total + 4.0 + own / 2
-        events += [(at / hidden, 0, k), (second, 1, k), (total, 2, k), (relay, 3, k), (relay + 2.6 + own / 2, 4, k)]
+    for k, (at, wide, inner_first) in enumerate(spans):
+        if inner_first:
+            inner_sum += 4.0 * wide / hidden
+            second = 0.6 + inner_sum + 2.6
+            total = second + 4.2 + 4.0 * wide / hidden
+        else:
+            outer_sum += 16.0 * wide / hidden
+            second = 1.0 + outer_sum + 4.2
+            total = second + 2.6 + 4.0 * wide / hidden
+        relay = total + 4.0 + 2.0 * wide / hidden
+        events += [(at / hidden, 0, k), (second, 1, k), (total, 2, k), (relay, 3, k), (relay + 3.0, 4, k)]
     return [(kind, k) for _, kind, k in sorted(events)]
 
 
@@ -260,9 +282,9 @@
     bias_ref, m_ref, n_ref, gain2_ref, clow = take(5)
     wload, cload, sload = take(3)
     gates_rs = Scatter(*take(5))
-    proj_rs = [Scatter(*take(5)) for _ in range(2 + 2 * heads)]
-    head_ag = [Gather(*take(2)) for _ in range(heads)]
-    ffn_rs = [Scatter(*take(5)) for _ in spans]
+    proj_rs = [Scatter(*take(5), i < 1 + 2 * heads) for i in range(2 + 2 * heads)]
+    head_ag = [Gather(*take(2), True) for _ in range(heads)]
+    ffn_rs = [Scatter(*take(5), span[2]) for span in spans]
     square_rs = Scatter(*take(5))
     ffn_ag = [Gather(*take(2)) for _ in spans]
     abuf, dbuf, mid_v, acc_v, cols_v, asem, dsem, turn = take(8)
@@ -301,21 +323,25 @@
     ]
     for load in small:
         load.start()
-    loads = []
-    for i, (src, dst, at, wide) in enumerate(chunks):
+    loads = {}
+    for i in [0, len(chunks) - 1, *range(1, len(chunks) - 1)]:
+        src, dst, at, wide = chunks[i]
         load = pltpu.make_async_copy(
             src.at[:, pl.ds(at, wide)], dst.at[:, pl.ds(at, wide)], wload.at[7 + i]
         )
         load.start()
-        loads.append(load)
+        loads[i] = load
     early[0].wait()
     early[1].wait()
     tok = tok_v[...].astype(F32)
     normed = (tok * gain1_v[...]).astype(BF16)
-    proj_queue = Queue([proj_rs[0], gates_rs, *proj_rs[1:]], turn.at[0], PROJ_WINDOW, PROJ_HAND)
-    for i, (_, dst, at, wide) in enumerate(chunks):
+    proj_queue = Queue([proj_rs[0], gates_rs, *proj_rs[1:-1]], turn.at[0], PROJ_WINDOW, PROJ_HAND)
+    last = len(chunks) - 1
+    turns = [0, last, *range(1, last)]
+    for i in turns:
+        _, dst, at, wide = chunks[i]
         loads[i].wait()
-        if i == len(chunks) - 1:
+        if i == turns[-1]:
             for h in range(heads):
                 for b in range(rows):
                     pltpu.make_async_copy(c_hbm.at[b, h], newc_ref.at[b, h], cload).start()
@@ -326,7 +352,7 @@
             for load in late:
                 load.start()
         out = jnp.dot(normed, dst[:, at : at + wide], preferred_element_type=F32)
-        put_part(proj_rs[i].part, out, 0, wide)
+        proj_rs[i].put(out, 0, wide)
         if i == 0:
             pl.semaphore_wait(barrier, count - 1 + lax.axis_size("tp") - 1)
             proj_queue.early(0)
@@ -335,9 +361,11 @@
                 normed, wg_v[...], (((1,), (1,)), ((), ())), preferred_element_type=F32
             )
             squares = jnp.sum(tok * tok, axis=1, keepdims=True)
-            put_part(gates_rs.part, jnp.broadcast_to(squares, (batch, LANES)), 0, LANES)
-            put_part(gates_rs.part, gates, 0, gate_cols)
+            gates_rs.put(jnp.broadcast_to(squares, (batch, LANES)), 0, LANES)
+            gates_rs.put(gates, 0, gate_cols)
             proj_queue.early(1)
+        elif i == last:
+            proj_rs[i].start()
         else:
             proj_queue.early(i + 1)
     proj_queue.late()
@@ -429,32 +457,36 @@
     for group in [gates_rs, *proj_rs, *head_ag]:
         group.settle()
     proj_queue.finish()
+    proj_rs[-1].drain()
     attn_mix = tp_total(abuf, asem)
     middle = (tok_v[...].astype(F32) + attn_mix).astype(BF16)
     mid_v[...] = middle
     mid = middle.astype(F32)
     squares = jnp.sum(mid * mid, axis=1, keepdims=True)
     normed = (mid * gain2_ref[...]).astype(BF16)
-    put_part(square_rs.part, jnp.broadcast_to(squares, (batch, LANES)), 0, LANES)
+    square_rs.put(jnp.broadcast_to(squares, (batch, LANES)), 0, LANES)
     late[1].wait()
     late[2].wait()
-    ffn_queue = Queue([square_rs, *ffn_rs], turn.at[1], FFN_WINDOW, FFN_HAND)
+    ffn_queue = Queue([square_rs, *[rs for rs in ffn_rs if rs.inner_first]], turn.at[1], FFN_WINDOW, FFN_HAND)
     scale2 = None
     for kind, k in ffn_order(spans):
-        at, wide = spans[k]
+        at, wide, inner_first = spans[k]
         half = padded(wide)
         if kind == 0:
             for j, weight in enumerate([wgf_v, wuf_v]):
                 out = lax.dot_general(
                     normed, weight[at : at + wide, :], (((1,), (1,)), ((), ())), preferred_element_type=F32
                 )
-                put_part(ffn_rs[k].part, out, j * half, wide)
+                ffn_rs[k].put(out, j * half, wide)
                 if half > wide:
                     fill = jnp.zeros((batch, half - wide), F32)
-                    put_part(ffn_rs[k].part, fill, j * half + wide, half - wide)
+                    ffn_rs[k].put(fill, j * half + wide, half - wide)
             if k == 0:
                 ffn_queue.early(0)
-            ffn_queue.early(k + 1)
+            if inner_first:
+                ffn_queue.early(ffn_queue.scatters.index(ffn_rs[k]))
+            else:
+                ffn_rs[k].start()
             if k == len(spans) - 1:
                 ffn_queue.late()
         elif kind == 1:
@@ -488,6 +520,9 @@
     for group in [square_rs, *ffn_rs, *ffn_ag]:
         group.settle()
     ffn_queue.finish()
+    for rs in ffn_rs:
+        if not rs.inner_first:
+            rs.drain()
     tp_settle(abuf, asem)
     down = tp_total(dbuf, dsem)
     mixed_ref[...] = (mid_v[...].astype(F32) + down).astype(BF16)
@@ -554,14 +589,16 @@
         sem((4,)),
     ]
     scratch += scatter_scratch(inner, outer, rows, LANES, F32)
-    for wide in chunks:
+    for wide in chunks[:-1]:
         scratch += scatter_scratch(inner, outer, rows, wide, BF16)
+    scratch += scatter_scratch(outer, inner, rows, chunks[-1], BF16)
     for _ in range(heads):
         scratch += gather_scratch(count, rows, value_size)
-    for _, wide in spans:
-        scratch += scatter_scratch(inner, outer, rows, 2 * padded(wide), BF16)
+    for _, wide, inner_first in spans:
+        firsts, seconds = (inner, outer) if inner_first else (outer, inner)
+        scratch += scatter_scratch(firsts, seconds, rows, 2 * padded(wide), BF16)
     scratch += scatter_scratch(inner, outer, rows, LANES, F32)
-    for _, wide in spans:
+    for _, wide, _ in spans:
         scratch += gather_scratch(count, rows, wide)
     scratch += [
         pltpu.VMEM((tps, batch, width), BF16),

time: 57.5 us -> 53 us (0.922)
  Pallas kernels: 56.7 us -> 52.3 us
    pallas_call x1, Pallas kernels: 53.3 us -> 48.8 us  [per_device(): pl.pallas_call(kernel, out_shape=kernel_outs, in_specs=[HBM_SPEC] * len(a...]
where the time goes in v4:
time: 53 us; the launch traced here: 52.9 us
  Pallas kernels  52.3 us (99%)
  between operations  0.65 us (1%)
    pallas_call x1, Pallas kernels, per_device(): pl.pallas_call(kernel, out_shape=kernel_outs, in_specs=[HBM_SPEC] * len(a...  48.8 us
    pallas_call x1, Pallas kernels, per_device(): pl.pallas_call(store_kernel, out_shape=kernel_outs, in_specs=[VMEM_SPEC]...  3.4 us

profile of v4, /device:TPU:1, one launch (start us, length us, event | category | flops | bytes accessed | tf_op | source)
XLA Modules:
  0.0 52.9 jit_solution(17425799249965284617)
XLA Ops:
  0.6 48.8 %layer.1 = (bf16[64,512]{1,0:T(8,128)(2,1)S(1)}, f32[8,2,512,256]{3,2,1,0:T(8,128)S(1)}, f32[8,2,256]{2,1,0:T(2,128)S(1)}, f32[2,8]{1,0:T(2,128)S(1)}) custom-call(bf16[64,512]{1,0:T(8,128)(2,1)} %refs_0_.1, f32[1,512]{1,0:T(1,128)} %bitcast.11, bf16[512,512]{1,0:T(8,128)(2,1)} %refs_2_.1, bf16[512,512]{1,0:T(8,128)(2,1)} %refs_3_.1, ...), custom_call_target="tpu_custom_call" | custom-call | tf_op jit(solution)/shard_map/layer/pallas_call | solution.py:623
  49.5 3.4 %store.1 = (bf16[64,512]{1,0:T(8,128)(2,1)}, f32[8,2,512,256]{3,2,1,0:T(8,128)}, f32[8,2,256]{2,1,0:T(2,128)}, f32[2,8]{1,0:T(2,128)}) custom-call(bf16[64,512]{1,0:T(8,128)(2,1)S(1)} %get-tuple-element.12.mixed_in, f32[8,2,512,256]{3,2,1,0:T(8,128)S(1)} %get-tuple-element.13.c_in, f32[8,2,256]{2,1,0:T(2,128)S(1)} %get-tuple-element.14.n_in, ...), custom_call_target="tpu_custom_call" | custom-call | tf_op jit(solution)/shard_map/store/pallas_call | solution.py:635

commit v5 on v4

--- a/solution.py
+++ b/solution.py
@@ -8,11 +8,9 @@
 norm_floor = 1e-05
 MESH = pl.DeviceIdType.MESH
 LANES = 128
-SPAN = 512
-EDGE = 256
-PROJ_WINDOW, PROJ_HAND = 6, 2
+PROJ_WINDOW, PROJ_HAND = 6, 4
 FFN_WINDOW, FFN_HAND = 3, 1
-OUTER_SPAN, OUTER_AT = 640, (1,)
+SPANS, OUTER_AT = (512, 640, 512, 512, 256), (1,)
 
 VMEM_ALL = 67043328
 ROOM = 4 * 1024 * 1024
@@ -241,10 +239,11 @@
 
 def hidden_spans(hidden):
     sizes = []
-    while hidden - sum(sizes) >= SPAN + EDGE:
-        sizes.append(OUTER_SPAN if len(sizes) in OUTER_AT else SPAN)
+    for wide in SPANS:
+        if hidden - sum(sizes) > wide:
+            sizes.append(wide)
     while hidden > sum(sizes):
-        sizes.append(min(EDGE, hidden - sum(sizes)))
+        sizes.append(min(SPANS[-1], hidden - sum(sizes)))
     return [(sum(sizes[:k]), wide, k not in OUTER_AT) for k, wide in enumerate(sizes)]
 
 
@@ -324,7 +323,7 @@
     for load in small:
         load.start()
     loads = {}
-    for i in [0, len(chunks) - 1, *range(1, len(chunks) - 1)]:
+    for i in [0, 1, len(chunks) - 1, *range(2, len(chunks) - 1)]:
         src, dst, at, wide = chunks[i]
         load = pltpu.make_async_copy(
             src.at[:, pl.ds(at, wide)], dst.at[:, pl.ds(at, wide)], wload.at[7 + i]
@@ -337,7 +336,7 @@
     normed = (tok * gain1_v[...]).astype(BF16)
     proj_queue = Queue([proj_rs[0], gates_rs, *proj_rs[1:-1]], turn.at[0], PROJ_WINDOW, PROJ_HAND)
     last = len(chunks) - 1
-    turns = [0, last, *range(1, last)]
+    turns = [0, 1, last, *range(2, last)]
     for i in turns:
         _, dst, at, wide = chunks[i]
         loads[i].wait()
@@ -441,9 +440,8 @@
             newc_ref[b, h] = (
                 keep_wide[b : b + 1, :] * newc_ref[b, h] + cols_v[h, :, b : b + 1] * keys[h][b : b + 1, :]
             )
-        if h == 0:
-            for ag in head_ag:
-                ag.relay()
+    for ag in head_ag:
+        ag.relay()
 
     late[0].wait()
     attn = None
@@ -469,7 +467,9 @@
     late[2].wait()
     ffn_queue = Queue([square_rs, *[rs for rs in ffn_rs if rs.inner_first]], turn.at[1], FFN_WINDOW, FFN_HAND)
     scale2 = None
-    for kind, k in ffn_order(spans):
+    order = ffn_order(spans)
+    seconds = [k for kind, k in order if kind == 1]
+    for kind, k in order:
         at, wide, inner_first = spans[k]
         half = padded(wide)
         if kind == 0:
@@ -491,7 +491,7 @@
                 ffn_queue.late()
         elif kind == 1:
             ffn_rs[k].second()
-            if k == 0:
+            if k == seconds[0]:
                 square_rs.second()
         elif kind == 2:
             if scale2 is None:

time: 53 us -> 52.6 us (level)
  no operation moved by 1% of the time
where the time goes in v5:
time: 52.6 us; the launch traced here: 52.5 us
  Pallas kernels  51.8 us (98%)
  between operations  0.65 us (1%)
    pallas_call x1, Pallas kernels, per_device(): pl.pallas_call(kernel, out_shape=kernel_outs, in_specs=[HBM_SPEC] * len(a...  48.4 us
    pallas_call x1, Pallas kernels, per_device(): pl.pallas_call(store_kernel, out_shape=kernel_outs, in_specs=[VMEM_SPEC]...  3.4 us

profile of v5, /device:TPU:1, one launch (start us, length us, event | category | flops | bytes accessed | tf_op | source)
XLA Modules:
  0.0 52.5 jit_solution(11228852847452897378)
XLA Ops:
  0.6 48.4 %layer.1 = (bf16[64,512]{1,0:T(8,128)(2,1)S(1)}, f32[8,2,512,256]{3,2,1,0:T(8,128)S(1)}, f32[8,2,256]{2,1,0:T(2,128)S(1)}, f32[2,8]{1,0:T(2,128)S(1)}) custom-call(bf16[64,512]{1,0:T(8,128)(2,1)} %refs_0_.1, f32[1,512]{1,0:T(1,128)} %bitcast.11, bf16[512,512]{1,0:T(8,128)(2,1)} %refs_2_.1, bf16[512,512]{1,0:T(8,128)(2,1)} %refs_3_.1, ...), custom_call_target="tpu_custom_call" | custom-call | tf_op jit(solution)/shard_map/layer/pallas_call | solution.py:623
  49.1 3.4 %store.1 = (bf16[64,512]{1,0:T(8,128)(2,1)}, f32[8,2,512,256]{3,2,1,0:T(8,128)}, f32[8,2,256]{2,1,0:T(2,128)}, f32[2,8]{1,0:T(2,128)}) custom-call(bf16[64,512]{1,0:T(8,128)(2,1)S(1)} %get-tuple-element.12.mixed_in, f32[8,2,512,256]{3,2,1,0:T(8,128)S(1)} %get-tuple-element.13.c_in, f32[8,2,256]{2,1,0:T(2,128)S(1)} %get-tuple-element.14.n_in, ...), custom_call_target="tpu_custom_call" | custom-call | tf_op jit(solution)/shard_map/store/pallas_call | solution.py:635

commit v6 on v5

--- a/solution.py
+++ b/solution.py
@@ -10,7 +10,7 @@
 LANES = 128
 PROJ_WINDOW, PROJ_HAND = 6, 4
 FFN_WINDOW, FFN_HAND = 3, 1
-SPANS, OUTER_AT = (512, 640, 512, 512, 256), (1,)
+SPANS, OUTER_AT = (512, 640, 512, 512, 320, 256), (1,)
 
 VMEM_ALL = 67043328
 ROOM = 4 * 1024 * 1024

time: 52.6 us -> 52.5 us (level)
  no operation moved by 1% of the time
where the time goes in v6:
time: 52.5 us; the launch traced here: 52.3 us
  Pallas kernels  51.7 us (98%)
  between operations  0.65 us (1%)
    pallas_call x1, Pallas kernels, per_device(): pl.pallas_call(kernel, out_shape=kernel_outs, in_specs=[HBM_SPEC] * len(a...  48.3 us
    pallas_call x1, Pallas kernels, per_device(): pl.pallas_call(store_kernel, out_shape=kernel_outs, in_specs=[VMEM_SPEC]...  3.4 us

profile of v6, /device:TPU:1, one launch (start us, length us, event | category | flops | bytes accessed | tf_op | source)
XLA Modules:
  0.0 52.3 jit_solution(6581609963933823749)
XLA Ops:
  0.6 48.3 %layer.1 = (bf16[64,512]{1,0:T(8,128)(2,1)S(1)}, f32[8,2,512,256]{3,2,1,0:T(8,128)S(1)}, f32[8,2,256]{2,1,0:T(2,128)S(1)}, f32[2,8]{1,0:T(2,128)S(1)}) custom-call(bf16[64,512]{1,0:T(8,128)(2,1)} %refs_0_.1, f32[1,512]{1,0:T(1,128)} %bitcast.11, bf16[512,512]{1,0:T(8,128)(2,1)} %refs_2_.1, bf16[512,512]{1,0:T(8,128)(2,1)} %refs_3_.1, ...), custom_call_target="tpu_custom_call" | custom-call | tf_op jit(solution)/shard_map/layer/pallas_call | solution.py:623
  48.9 3.4 %store.1 = (bf16[64,512]{1,0:T(8,128)(2,1)}, f32[8,2,512,256]{3,2,1,0:T(8,128)}, f32[8,2,256]{2,1,0:T(2,128)}, f32[2,8]{1,0:T(2,128)}) custom-call(bf16[64,512]{1,0:T(8,128)(2,1)S(1)} %get-tuple-element.12.mixed_in, f32[8,2,512,256]{3,2,1,0:T(8,128)S(1)} %get-tuple-element.13.c_in, f32[8,2,256]{2,1,0:T(2,128)S(1)} %get-tuple-element.14.n_in, ...), custom_call_target="tpu_custom_call" | custom-call | tf_op jit(solution)/shard_map/store/pallas_call | solution.py:635
